TPU v7x, 128 devices: a whole 4x4x4 slice. The times are simulated.
128 devices in a mesh: fs: 16 (over z, y), tp: 8 (over x, core).
Axes of the slice: x: 4, y: 4, z: 4, core: 2. Of those that a mesh axis runs over, the one named last changes fastest.
Arguments:
- tokens: bfloat16 [32, 384, 2048], P('fs', None, 'tp'), may hold values from -34 to 34
- mix_gain: float32 [2048], replicated, may hold values from 0.1 to 1.9
- w_bgate: float32 [2048, 2048], P('fs', 'tp'), may hold values from -0.125 to 0.125
- w_cgate: float32 [2048, 2048], P('fs', 'tp'), may hold values from -0.125 to 0.125
- w_value: float32 [2048, 2048], P('fs', 'tp'), may hold values from -0.125 to 0.125
- in_scale: float32 [3, 2048], P(None, 'tp'), may hold values from 0.5 to 2
- mix_taps: float32 [3, 2048], P(None, 'tp'), may hold values from -3.5 to 3.5
- w_mixout: float32 [2048, 2048], P('tp', 'fs'), may hold values from -0.125 to 0.125
- mixout_scale: float32 [1, 2048], P(None, 'fs'), may hold values from 0.5 to 2
- ffn_gain: float32 [2048], replicated, may hold values from 0.1 to 1.9
- w_upgate: float32 [2048, 5632], P('fs', 'tp'), may hold values from -0.125 to 0.125
- w_upval: float32 [2048, 5632], P('fs', 'tp'), may hold values from -0.125 to 0.125
- up_scale: float32 [2, 5632], P(None, 'tp'), may hold values from 0.5 to 2
- ffn_taps: float32 [2, 3, 5632], P(None, None, 'tp'), may hold values from -3.5 to 3.5
- w_down: float32 [5632, 2048], P('tp', 'fs'), may hold values from -0.078125 to 0.078125
- down_scale: float32 [1, 2048], P(None, 'fs'), may hold values from 0.5 to 2
Outputs:
- layer_out: bfloat16 [32, 384, 2048], P('fs', None, 'tp')
All inputs are finite; a program needn't handle non-finite values.
Results may differ from a plain program's by a relative error of at most 0.015.
Values may be sent and summed in bfloat16 or wider, within the bound.
A program may use at most 64 MiB of HBM per device.

v0:
```python
import jax
import jax.numpy as jnp
from jax import lax
from jax.sharding import Mesh
from jax.sharding import PartitionSpec as P

TP = ("tp_0", "tp_1")


EPS = 1e-06


def copy_for_each(value, axis):
    peers = lax.axis_size(axis)
    return lax.all_to_all(
        jnp.broadcast_to(value[None], (peers, *value.shape)), axis, 0, 0, tiled=True
    )


def joined_along(parts, dim):
    shape = list(parts.shape[1:])
    shape[dim] *= parts.shape[0]
    return jnp.moveaxis(parts, 0, dim).reshape(shape)


def gather_axes(value, axes, dim):
    far, near = axes
    first = copy_for_each(value, far)
    parts = jnp.swapaxes(copy_for_each(first, near), 0, 1)
    return joined_along(parts.reshape(-1, *value.shape), dim)


def in_one_piece(arrays, axis, dim, along):
    widths = [a.shape[along] for a in arrays]
    both = jnp.concatenate(arrays, axis=along)
    out = lax.all_gather(both, axis, axis=dim, tiled=True)
    return tuple(jnp.split(out, [sum(widths[:k]) for k in range(1, len(widths))], axis=along))


def collect(value, axis, dim):
    parts = copy_for_each(value, axis)
    return joined_along(parts, dim)


def split_up(value, dim, peers):
    before, after = (value.shape[:dim], value.shape[dim + 1 :])
    return jnp.moveaxis(value.reshape(*before, peers, -1, *after), dim, 0)


def sum_at_owner(value, axis, dim):
    peers = lax.axis_size(axis)
    parts = lax.all_to_all(split_up(value, dim, peers), axis, 0, 0, tiled=True)
    return jnp.sum(parts.astype(jnp.float32), axis=0)


def causal_taps(values, taps):
    length = values.shape[1]
    kernel = taps.shape[0]
    padded = jnp.pad(values, ((0, 0), (kernel - 1, 0), (0, 0)))
    result = jnp.zeros(values.shape, jnp.float32)
    for offset in range(kernel):
        result = result + padded[:, offset : offset + length] * taps[offset]
    return result


def normed_rows(shard, gain):
    gathered = gather_axes(shard, ("tp_0", "tp_1"), 2)
    floats = gathered.astype(jnp.float32)
    factor = lax.rsqrt(jnp.mean(floats * floats, axis=-1, keepdims=True) + EPS)
    result = (floats * factor * gain).astype(jnp.bfloat16)
    return result.reshape(-1, result.shape[-1])


def scaled_columns(piece, acts, scales):
    return (jnp.dot(acts, piece, preferred_element_type=jnp.float32) * scales).astype(jnp.bfloat16)


def dot_rows(inputs, matrix):
    return jnp.dot(inputs, matrix, preferred_element_type=jnp.float32)


def on_device(
    tokens,
    mix_gain,
    w_bgate,
    w_cgate,
    w_value,
    in_scale,
    mix_taps,
    w_mixout,
    mixout_scale,
    ffn_gain,
    w_upgate,
    w_upval,
    up_scale,
    ffn_taps,
    w_down,
    down_scale,
):
    seq_count, length, own_width = tokens.shape
    row_count = seq_count * length
    ff_width = w_upgate.shape[1]
    mix_scales, down_scales = in_one_piece((mixout_scale, down_scale), "fs", 1, 0)
    normed = normed_rows(tokens, mix_gain)
    bgate_rows = w_bgate.astype(jnp.bfloat16)
    cgate_rows = w_cgate.astype(jnp.bfloat16)
    value_rows = w_value.astype(jnp.bfloat16)
    bgate_full, cgate_full, value_full = in_one_piece(
        (bgate_rows, cgate_rows, value_rows), "fs", 0, 1
    )
    bgate = dot_rows(normed, bgate_full)
    cgate = dot_rows(normed, cgate_full)
    value = dot_rows(normed, value_full)
    bgate = bgate * in_scale[0]
    inner = cgate * in_scale[1] * (value * in_scale[2])
    convolved = causal_taps(inner.reshape(seq_count, length, own_width), mix_taps)
    gated = (
        (bgate.reshape(seq_count, length, own_width) * convolved)
        .astype(jnp.bfloat16)
        .reshape(row_count, own_width)
    )
    mix_terms = scaled_columns(
        collect(w_mixout.astype(jnp.bfloat16), "fs", 1), acts=gated, scales=mix_scales
    )
    mix = sum_at_owner(mix_terms.astype(jnp.float32).astype(jnp.bfloat16), TP, 1)
    resid = (tokens.reshape(row_count, own_width).astype(jnp.float32) + mix).astype(jnp.bfloat16)
    normed_ffn = normed_rows(resid.reshape(seq_count, length, own_width), ffn_gain)
    upgate_rows = w_upgate.astype(jnp.bfloat16)
    upval_rows = w_upval.astype(jnp.bfloat16)
    upgate_full, upval_full = in_one_piece((upgate_rows, upval_rows), "fs", 0, 1)
    gate_pre = dot_rows(normed_ffn, upgate_full)
    val_pre = dot_rows(normed_ffn, upval_full)
    gate_pre = (gate_pre * up_scale[0]).reshape(seq_count, length, ff_width)
    val_pre = (val_pre * up_scale[1]).reshape(seq_count, length, ff_width)
    gate_conv = causal_taps(gate_pre, ffn_taps[0])
    val_conv = causal_taps(val_pre, ffn_taps[1])
    active = (jax.nn.silu(gate_conv) * val_conv).astype(jnp.bfloat16).reshape(row_count, ff_width)
    down_terms = scaled_columns(
        lax.all_gather(w_down.astype(jnp.bfloat16), "fs", axis=1, tiled=True),
        acts=active,
        scales=down_scales,
    )
    ffn = sum_at_owner(down_terms.astype(jnp.float32).astype(jnp.bfloat16), TP, 1)
    layer_out = (resid.astype(jnp.float32) + ffn).astype(jnp.bfloat16)
    return layer_out.reshape(seq_count, length, own_width)


def solution(mesh):
    split = Mesh(mesh.devices.reshape(mesh.shape["fs"], 4, 2), ("fs", "tp_0", "tp_1"))
    return jax.shard_map(
        on_device,
        mesh=split,
        in_specs=(
            P("fs", None, TP),
            P(),
            P("fs", TP),
            P("fs", TP),
            P("fs", TP),
            P(None, TP),
            P(None, TP),
            P(TP, "fs"),
            P(None, "fs"),
            P(),
            P("fs", TP),
            P("fs", TP),
            P(None, TP),
            P(None, None, TP),
            P(TP, "fs"),
            P(None, "fs"),
        ),
        out_specs=P("fs", None, TP),
        check_vma=False,
    )
```

profile of v0, /device:TPU:1, one launch (start us, length us, event | category | flops | bytes accessed | tf_op | source)
XLA Modules:
  0.0 236.2 jit_solution(5192973398309712836)
XLA Ops:
  6.5 1.0 convert_element_type.128
  7.5 0.9 convert_element_type.129
  8.4 0.9 convert_element_type.130
  9.3 0.7 pad_maximum_fusion.1
  10.0 0.0 all-gather.4.cloned.1.call-update
  10.0 0.0 all-gather.6.cloned.1.call-start
  10.1 1.0 convert_element_type.144
  11.1 1.0 convert_element_type.145
  12.1 0.0 copy-start.2
  12.1 0.0 copy-start.12
  12.2 0.8 pad_maximum_fusion
  12.9 0.0 all-gather.6.cloned.1.call-update
  13.0 1.3 broadcast_in_dim.10
  14.2 4.8 %all-to-all-start = ((bf16[4,2,384,256]{3,2,1,0:T(8,128)(2,1)}), bf16[4,2,384,256]{3,2,1,0:T(8,128)(2,1)S(1)}, u32[]{:S(2)}, u32[]{:S(2)}) async-start(bf16[4,2,384,256]{3,2,1,0:T(8,128)(2,1)} %broadcast_in_dim.10), calls=%async_computation | async-start | bytes 3145728 | tf_op jit(solution)/shard_map/all_to_all | solution.py:15
  19.1 0.7 copy.36
  19.8 20.8 %all_gather.13 = f32[2,2048]{1,0:T(2,128)S(1)} all-gather(f32[2,128]{1,0:T(2,128)S(1)} %pad_maximum_fusion.2), channel_id=1, replica_groups=mesh['fs'=16,'tp_0'=4,'tp_1'=2] {'fs'}, dimensions={1}, use_global_device_ids=true | all-gather | bytes 17408 | tf_op jit(solution)/shard_map/all_gather | solution.py:36
  40.7 0.6 fusion.27
  41.3 0.6 fusion.26
  41.9 0.6 fusion.25
  42.5 0.3 broadcast_in_dim.11
  42.8 11.0 %all_to_all.35 = bf16[2,4,2,384,256]{4,3,2,1,0:T(8,128)(2,1)S(1)} all-to-all(bf16[2,4,2,384,256]{4,3,2,1,0:T(8,128)(2,1)S(1)} %broadcast_in_dim.11), channel_id=1, replica_groups=mesh['fs'=16,'tp_0'=4,'tp_1'=2] {'tp_1'}, dimensions={0} | all-to-all | bytes 6291456 | tf_op jit(solution)/shard_map/all_to_all | solution.py:15
  53.8 1.1 broadcast_in_dim.12
  54.9 4.5 %all-to-all-start.2 = ((bf16[16,256,128]{1,2,0:T(8,128)(2,1)}), bf16[16,256,128]{1,2,0:T(8,128)(2,1)}, u32[]{:S(2)}, u32[]{:S(2)}) async-start(bf16[16,256,128]{1,2,0:T(8,128)(2,1)} %broadcast_in_dim.12), calls=%async_computation.2 | async-start | bytes 2097152 | tf_op jit(solution)/shard_map/all_to_all | solution.py:15
  59.4 0.7 copy_convert_fusion.1
  60.1 3.6 %copy.35 = f32[2,384,8,256]{3,2,1,0:T(8,128)S(1)} copy(f32[2,384,8,256]{3,1,0,2:T(8,128)S(1)} %bitcast.65) | data formatting | bytes 12582912 | tf_op jit(solution)/shard_map/convert_element_type | solution.py:68
  63.8 5.7 %copy.51 = f32[96,8,8,256]{3,1,2,0:T(8,128)} copy(f32[96,8,8,256]{3,2,1,0:T(8,128)S(1)} %bitcast.63) | data formatting | bytes 12582912
  69.5 0.7 multiply_reduce_fusion.1
  70.2 3.6 %multiply_convert_fusion.3 = bf16[768,2048]{1,0:T(8,128)(2,1)S(1)} fusion(f32[768,2048]{1,0:T(8,128)} %bitcast.62, f32[2048]{0:T(1024)} %param.17, f32[768]{0:T(1024)S(1)} %rsqrt.23), kind=kLoop, calls=%fused_computation.7 | loop fusion | flops 4718592 | bytes 9448448 | tf_op jit(solution)/shard_map/convert_element_type | solution.py:70
  73.8 0.0 all-gather.4.cloned.1.call-done
  73.8 2.4 %convolution_multiply_fusion.1 = f32[768,256]{1,0:T(8,128)S(1)} fusion(bf16[768,2048]{1,0:T(8,128)(2,1)S(1)} %multiply_convert_fusion.3, bf16[2048,768]{1,0:T(8,128)(2,1)} %all-gather.4.cloned.1.call-done, f32[256]{0:T(256)} %bitcast.89), kind=kOutput, calls=%fused_computation.36 | convolution fusion | flops 805502976 | bytes 4981760 | tf_op jit(solution)/shard_map/dot_general | solution.py:79
  76.2 1.0 convolution_multiply_fusion.2
  77.3 1.0 fusion.20
  78.3 0.3 multiply_convert_fusion.4
  78.6 2.5 %multiply_convert_fusion.2 = bf16[768,2048]{1,0:T(8,128)(2,1)S(1)} fusion(bf16[768,256]{1,0:T(8,128)(2,1)S(1)} %bitcast.78, bf16[256,2048]{0,1:T(8,128)(2,1)} %bitcast.13, f32[2048]{0:T(1024)S(1)} %bitcast.82), kind=kOutput, calls=%fused_computation.6 | convolution fusion | flops 808452096 | bytes 4595712 | tf_op jit(solution)/shard_map/dot_general | solution.py:75
  81.1 1.8 copy.64
  82.9 5.5 %all-to-all-start.3 = ((bf16[8,768,256]{2,1,0:T(8,128)(2,1)}), bf16[8,768,256]{2,1,0:T(8,128)(2,1)S(1)}, u32[]{:S(2)}, u32[]{:S(2)}) async-start(bf16[8,768,256]{2,1,0:T(8,128)(2,1)} %bitcast.61), calls=%async_computation.3 | async-start | bytes 6291456 | tf_op jit(solution)/shard_map/all_to_all | solution.py:52
  88.4 1.7 convert_element_type.147
  90.0 0.0 all-gather.8.cloned.1.call-update
  90.1 35.7 %all-to-all-done.3 = bf16[8,768,256]{2,1,0:T(8,128)(2,1)S(1)} async-done(((bf16[8,768,256]{2,1,0:T(8,128)(2,1)}), bf16[8,768,256]{2,1,0:T(8,128)(2,1)S(1)}, u32[]{:S(2)}, u32[]{:S(2)}) %all-to-all-start.3) | async-done | bytes 3145760 | tf_op jit(solution)/shard_map/all_to_all | solution.py:52
  125.8 0.4 convert_reduce_fusion.1
  126.3 0.1 add_convert_fusion.1
  126.4 1.3 broadcast_in_dim.13
  127.6 3.6 %all-to-all-start.4 = ((bf16[4,2,384,256]{3,2,1,0:T(8,128)(2,1)}), bf16[4,2,384,256]{3,2,1,0:T(8,128)(2,1)S(1)}, u32[]{:S(2)}, u32[]{:S(2)}) async-start(bf16[4,2,384,256]{3,2,1,0:T(8,128)(2,1)} %broadcast_in_dim.13), calls=%async_computation.4 | async-start | bytes 3145728 | tf_op jit(solution)/shard_map/all_to_all | solution.py:15
  131.2 0.1 slice_reduce_fusion.6
  131.3 19.7 %all-to-all-done.4 = bf16[4,2,384,256]{3,2,1,0:T(8,128)(2,1)S(1)} async-done(((bf16[4,2,384,256]{3,2,1,0:T(8,128)(2,1)}), bf16[4,2,384,256]{3,2,1,0:T(8,128)(2,1)S(1)}, u32[]{:S(2)}, u32[]{:S(2)}) %all-to-all-start.4) | async-done | bytes 1572896 | tf_op jit(solution)/shard_map/all_to_all | solution.py:15
  151.0 0.3 broadcast_in_dim.14
  151.3 7.7 %all_to_all.36 = bf16[2,4,2,384,256]{4,3,2,1,0:T(8,128)(2,1)S(1)} all-to-all(bf16[2,4,2,384,256]{4,3,2,1,0:T(8,128)(2,1)S(1)} %broadcast_in_dim.14), channel_id=1, replica_groups=mesh['fs'=16,'tp_0'=4,'tp_1'=2] {'tp_1'}, dimensions={0} | all-to-all | bytes 6291456 | tf_op jit(solution)/shard_map/all_to_all | solution.py:15
  159.0 0.7 copy_convert_fusion
  159.7 3.6 %copy.39 = f32[2,384,8,256]{3,2,1,0:T(8,128)S(1)} copy(f32[2,384,8,256]{3,1,0,2:T(8,128)S(1)} %bitcast.66) | data formatting | bytes 12582912 | tf_op jit(solution)/shard_map/convert_element_type | solution.py:68
  163.4 5.7 %copy.52 = f32[96,8,8,256]{3,1,2,0:T(8,128)} copy(f32[96,8,8,256]{3,2,1,0:T(8,128)S(1)} %bitcast.64) | data formatting | bytes 12582912
  169.1 0.7 multiply_reduce_fusion
  169.8 0.0 all-gather.6.cloned.1.call-done
  169.8 6.4 %fusion.14 = f32[768,704]{0,1:T(8,128)S(1)} fusion(bf16[2048,1408]{0,1:T(8,128)(2,1)} %all-gather.6.cloned.1.call-done, f32[704]{0:T(1024)S(1)} %get-tuple-element.11, f32[768,2048]{1,0:T(8,128)} %bitcast.69, f32[2048]{0:T(1024)S(1)} %copy-done.16, f32[768]{0:T(1024)S(1)} %rsqrt.25), kind=kOutput, calls=%fused_computation.32 | convolution fusion | flops 2219851776 | bytes 11351808 | tf_op jit(solution)/shard_map/dot_general | solution.py:79
  176.3 0.4 copy-done.14
  176.7 2.8 %fusion.17 = f32[768,704]{0,1:T(8,128)S(1)} fusion(bf16[2048,1408]{0,1:T(8,128)(2,1)S(1)} %copy-done.14, f32[704]{0:T(1024)S(1)} %get-tuple-element.12, f32[768,2048]{1,0:T(8,128)S(1)} %bitcast.72, f32[2048]{0:T(1024)S(1)} %copy-done.16, f32[768]{0:T(1024)S(1)} %rsqrt.25), kind=kOutput, calls=%fused_computation.33 | convolution fusion | flops 2219851776 | bytes 11354112 | tf_op jit(solution)/shard_map/dot_general | solution.py:79
  179.5 0.3 copy_bitcast_fusion
  179.8 3.3 %fusion.21 = bf16[2,88,8,384]{3,2,1,0:T(8,128)(2,1)S(1)} fusion(f32[2,384,704]{1,2,0:T(8,128)S(1)} %get-tuple-element.21, f32[704]{0:T(1024)S(1)} %get-tuple-element.9, f32[704]{0:T(1024)S(1)} %get-tuple-element.10, f32[704]{0:T(1024)S(1)} %get-tuple-element.6, f32[2,384,704]{1,2,0:T(8,128)S(1)} %get-tuple-element.22, f32[704]{0:T(1024)S(1)} %get-tuple-element.7, ...), kind=kLoop, calls=%fused_computation.38 | loop fusion | flops 8650752 | bytes 5423616
  183.1 0.1 copy.50
  183.2 0.0 all-gather.8.cloned.1.call-done
  183.2 4.7 %multiply_convert_fusion = bf16[768,2048]{1,0:T(8,128)(2,1)S(1)} fusion(bf16[768,704]{0,1:T(8,128)(2,1)S(1)} %bitcast.79, bf16[704,2048]{1,0:T(8,128)(2,1)} %all-gather.8.cloned.1.call-done, f32[2048]{0:T(1024)S(1)} %bitcast.83), kind=kOutput, calls=%fused_computation.3 | convolution fusion | flops 2217738240 | bytes 7118848 | tf_op jit(solution)/shard_map/dot_general | solution.py:75
  187.9 0.2 copy.63
  188.2 40.2 %all_to_all.37 = bf16[8,768,256]{2,1,0:T(8,128)(2,1)S(1)} all-to-all(bf16[8,768,256]{2,1,0:T(8,128)(2,1)S(1)} %bitcast.68), channel_id=1, replica_groups=mesh['fs'=16,'tp_0'=4,'tp_1'=2] {'tp_0','tp_1'}, dimensions={0} | all-to-all | bytes 6291456 | tf_op jit(solution)/shard_map/all_to_all | solution.py:52
  228.4 0.4 convert_reduce_fusion
  228.8 0.9 add_convert_fusion
  (47 shorter events, 0.2 us)
Async XLA Ops:
  6.5 6.4 %copy-start = (bf16[2,384,256]{2,1,0:T(8,128)(2,1)S(1)}, bf16[2,384,256]{2,1,0:T(8,128)(2,1)}, u32[]{:S(2)}) copy-start(bf16[2,384,256]{2,1,0:T(8,128)(2,1)} %param.16) | copy-start | bytes 1179652
  6.5 67.3 %all-gather.4.cloned.1.call-start = ((), (), s32[]{:S(2)}) async-start(), calls=%async_computation.7 | async-start | bytes 3342336 | tf_op jit(solution)/shard_map/all_gather | solution.py:36
  10.0 159.8 %all-gather.6.cloned.1.call-start = ((), (), s32[]{:S(2)}) async-start(), calls=%async_computation.8 | async-start | bytes 6127616 | tf_op jit(solution)/shard_map/all_gather | solution.py:36
  12.1 6.9 %copy-start.2 = (f32[256,128]{1,0:T(8,128)S(1)}, f32[256,128]{1,0:T(8,128)}, u32[]{:S(2)}) copy-start(f32[256,128]{1,0:T(8,128)} %param.23) | copy-start | bytes 393220
  12.1 7.7 %copy-start.12 = (f32[1,128]{1,0:T(1,128)S(1)}, f32[1,128]{1,0:T(1,128)}, u32[]{:S(2)}) copy-start(f32[1,128]{1,0:T(1,128)} %param.31) | copy-start | bytes 1540
  12.1 7.7 %copy-start.13 = (f32[1,128]{1,0:T(1,128)S(1)}, f32[1,128]{1,0:T(1,128)}, u32[]{:S(2)}) copy-start(f32[1,128]{1,0:T(1,128)} %param.24) | copy-start | bytes 1540
  12.1 28.5 %copy-start.8 = (f32[3,256]{1,0:T(4,128)S(1)}, f32[3,256]{1,0:T(4,128)}, u32[]{:S(2)}) copy-start(f32[3,256]{1,0:T(4,128)} %param.21) | copy-start | bytes 9220
  12.2 29.1 %copy-start.9 = (f32[3,256]{1,0:T(4,128)S(1)}, f32[3,256]{1,0:T(4,128)}, u32[]{:S(2)}) copy-start(f32[3,256]{1,0:T(4,128)} %param.22) | copy-start | bytes 9220
  14.2 28.3 %all-to-all-start = ((bf16[4,2,384,256]{3,2,1,0:T(8,128)(2,1)}), bf16[4,2,384,256]{3,2,1,0:T(8,128)(2,1)S(1)}, u32[]{:S(2)}, u32[]{:S(2)}) async-start(bf16[4,2,384,256]{3,2,1,0:T(8,128)(2,1)} %broadcast_in_dim.10), calls=%async_computation | async-start | bytes 3145728 | tf_op jit(solution)/shard_map/all_to_all | solution.py:15
  42.8 11.0 %copy-start.1 = (bf16[256,128]{0,1:T(8,128)(2,1)S(1)}, bf16[256,128]{0,1:T(8,128)(2,1)}, u32[]{:S(2)}) copy-start(bf16[256,128]{0,1:T(8,128)(2,1)} %copy.36) | copy-start | bytes 196612
  54.9 23.7 %all-to-all-start.2 = ((bf16[16,256,128]{1,2,0:T(8,128)(2,1)}), bf16[16,256,128]{1,2,0:T(8,128)(2,1)}, u32[]{:S(2)}, u32[]{:S(2)}) async-start(bf16[16,256,128]{1,2,0:T(8,128)(2,1)} %broadcast_in_dim.12), calls=%async_computation.2 | async-start | bytes 2097152 | tf_op jit(solution)/shard_map/all_to_all | solution.py:15
  73.8 2.4 %copy-start.11 = (f32[1,256]{1,0:T(1,128)S(1)}, f32[1,256]{1,0:T(1,128)}, u32[]{:S(2)}) copy-start(f32[1,256]{1,0:T(1,128)} %get-tuple-element.19) | copy-start | bytes 3076
  73.8 2.4 %copy-start.15 = (bf16[2048,768]{1,0:T(8,128)(2,1)S(1)}, bf16[2048,768]{1,0:T(8,128)(2,1)}, u32[]{:S(2)}) copy-start(bf16[2048,768]{1,0:T(8,128)(2,1)} %all-gather.4.cloned.1.call-done) | copy-start | bytes 9437188
  76.2 1.0 copy-start.10
  77.3 1.0 copy-start.6
  77.3 1.0 copy-start.7
  82.9 42.9 %all-to-all-start.3 = ((bf16[8,768,256]{2,1,0:T(8,128)(2,1)}), bf16[8,768,256]{2,1,0:T(8,128)(2,1)S(1)}, u32[]{:S(2)}, u32[]{:S(2)}) async-start(bf16[8,768,256]{2,1,0:T(8,128)(2,1)} %bitcast.61), calls=%async_computation.3 | async-start | bytes 6291456 | tf_op jit(solution)/shard_map/all_to_all | solution.py:52
  88.4 94.8 %all-gather.8.cloned.1.call-start = ((), (), s32[]{:S(2)}) async-start(), calls=%async_computation.9 | async-start | bytes 3063808 | tf_op jit(solution)/shard_map/all_gather | solution.py:139
  126.2 5.0 %copy-start.5 = (f32[2,704]{1,0:T(2,128)S(1)}, f32[2,704]{1,0:T(2,128)}, u32[]{:S(2)}) copy-start(f32[2,704]{1,0:T(2,128)} %param.28) | copy-start | bytes 16900
  126.2 5.0 %copy-start.3 = (f32[2,3,704]{2,0,1:T(2,128)S(1)}, f32[2,3,704]{2,0,1:T(2,128)}, u32[]{:S(2)}) copy-start(f32[2,3,704]{2,0,1:T(2,128)} %param.29) | copy-start | bytes 50692
  127.6 23.4 %all-to-all-start.4 = ((bf16[4,2,384,256]{3,2,1,0:T(8,128)(2,1)}), bf16[4,2,384,256]{3,2,1,0:T(8,128)(2,1)S(1)}, u32[]{:S(2)}, u32[]{:S(2)}) async-start(bf16[4,2,384,256]{3,2,1,0:T(8,128)(2,1)} %broadcast_in_dim.13), calls=%async_computation.4 | async-start | bytes 3145728 | tf_op jit(solution)/shard_map/all_to_all | solution.py:15
  169.1 0.8 copy-start.16
  169.1 7.2 %slice-start = ((s8[6291456]{0:T(1024)(128)(4,1)}), s8[2097152]{0:T(1024)(128)(4,1)S(1)}, s32[]{:S(2)}) async-start(s8[6291456]{0:T(1024)(128)(4,1)} %bitcast.70), calls=%async_computation.10 | async-start | bytes 4194304
  169.8 6.5 %slice-start.1 = ((s8[6291456]{0:T(1024)(128)(4,1)}), s8[4194304]{0:T(1024)(128)(4,1)S(1)}, s32[]{:S(2)}) async-start(s8[6291456]{0:T(1024)(128)(4,1)} %bitcast.70), calls=%async_computation.11 | async-start | bytes 8388608
  169.8 6.9 %copy-start.14 = (bf16[2048,1408]{0,1:T(8,128)(2,1)S(1)}, bf16[2048,1408]{0,1:T(8,128)(2,1)}, u32[]{:S(2)}) copy-start(bf16[2048,1408]{0,1:T(8,128)(2,1)} %all-gather.6.cloned.1.call-done) | copy-start | bytes 17301508
  179.8 3.4 %copy-start.4 = (f32[1,2048]{1,0:T(1,128)S(1)}, f32[1,2048]{1,0:T(1,128)}, u32[]{:S(2)}) copy-start(f32[1,2048]{1,0:T(1,128)} %get-tuple-element.13) | copy-start | bytes 24580
Sparse Core Ops, SparseCore 0:
  10.2 50.5 all-gather.3
  62.9 62.3 all-gather.5
  127.4 49.9 all-gather.7
where the time goes:
time: 237 us; the launch traced here: 236 us
  blocking collectives  79.8 us (34%)
  waiting for transfers between devices  55.6 us (23%)
  local copies, waits for them, and re-layouts  28.5 us (12%)
  matrix products  20.7 us (9%)
  other arithmetic  19.7 us (8%)
  starting transfers between devices  18.4 us (8%)
  between operations  13.6 us (6%)
    all_to_all x1, blocking collectives, sum_at_owner(): parts = lax.all_to_all(split_up(value, dim, peers), axis, 0, 0, tiled=True)  40.2 us
    all_to_all x1, waiting for transfers between devices, sum_at_owner(): parts = lax.all_to_all(split_up(value, dim, peers), axis, 0, 0, tiled=True)  35.7 us
    all_gather x1, blocking collectives, in_one_piece(): out = lax.all_gather(both, axis, axis=dim, tiled=True)  20.8 us
    all_to_all x3, waiting for transfers between devices, copy_for_each(): lax.all_to_all(jnp.broadcast_to(value[None], (peers, *value.shape)), axis...  19.7 us
    all_to_all x2, blocking collectives, copy_for_each(): lax.all_to_all(jnp.broadcast_to(value[None], (peers, *value.shape)), axis...  18.7 us
    dot_general x5, matrix products, dot_rows(): return jnp.dot(inputs, matrix, preferred_element_type=jnp.float32)  13.5 us
    all_to_all x3, starting transfers between devices, copy_for_each(): lax.all_to_all(jnp.broadcast_to(value[None], (peers, *value.shape)), axis...  12.9 us
    unnamed x40, local copies, waits for them, and re-layouts  11.9 us
  transfers between devices with their start and end apart: 7, of which 2 were waited for; matrix products, arithmetic and copies ran while one was open for 25% of the time, Pallas kernels for 0%

commit v1 on v0

v1 whole, which is shorter than its diff:
```python
import functools

import jax
import jax.numpy as jnp
from jax import lax
from jax.experimental import pallas as pl
from jax.experimental.pallas import tpu as pltpu
from jax.sharding import PartitionSpec as P

EPS = 1e-06
BF = jnp.bfloat16
F32 = jnp.float32
SEQ = 384
HALF = SEQ // 2
D = 2048
W = 256
ROUNDS = 13


def kernel(
    tok, mgain, wb, wc, wv, insc, mtaps, wm, msc, fgain, wug, wuv, upsc, ftaps, wd, dsc,
    out,
    g_in, g_mo, g_up, g_ul, g_dn, g_dl,
    tfull, rfull, cbuf, gated, active, tfac, rfac,
    sb, rb, keep, fbuf, nbuf, rf, rn,
    y_send, y_recv, a_send, a_recv, r_send, r_recv,
):
    fs = lax.axis_index("fs")
    tp = lax.axis_index("tp")
    z, y = fs // 4, fs % 4
    x, core = tp // 2, tp % 2
    xp, xm, xf = (x + 1) % 4, (x + 3) % 4, (x + 2) % 4
    dev_xp = (fs, xp * 2 + core)
    dev_xm = (fs, xm * 2 + core)
    dev_sib = (fs, x * 2 + 1 - core)
    dev_axis = (
        ((z * 4 + (y + 1) % 4, tp), (z * 4 + (y + 3) % 4, tp)),
        ((((z + 1) % 4) * 4 + y, tp), (((z + 3) % 4) * 4 + y, tp)),
    )
    pos = (y, z)
    started = []

    def send(src, dst, ssem, rsem, dev):
        copy = pltpu.make_async_remote_copy(
            src_ref=src, dst_ref=dst, send_sem=ssem, recv_sem=rsem,
            device_id=dev, device_id_type=pl.DeviceIdType.MESH,
        )
        copy.start()
        started.append(copy)

    def arrived(dst, rsem):
        pltpu.make_async_copy(dst, dst, rsem).wait()

    barrier = pltpu.get_barrier_semaphore()
    for dev in (*dev_axis[0], *dev_axis[1], dev_xp, dev_xm, dev_sib):
        pl.semaphore_signal(barrier, inc=1, device_id=dev, device_id_type=pl.DeviceIdType.MESH)

    def rounded(w):
        return w.astype(BF).astype(F32)

    def column(gain):
        return jnp.broadcast_to(gain[pl.ds(fs, 1), :], (128, 128)).T

    mcol = column(mgain)
    mcol2 = jnp.concatenate([mcol, mcol], axis=1)
    for k, (w, row) in enumerate(((wc, 1), (wv, 2), (wb, 0))):
        g_in[k, z, y] = (rounded(w[...]) * mcol2 * insc[row : row + 1, :]).astype(BF)
    g_mo[0, z, y] = (rounded(wm[...]) * msc[...]).astype(BF)
    fcol = column(fgain)
    for j in range(5):
        cols = slice(128 * j, 128 * j + 128)
        g_up[j, z, y, :, 0:128] = (rounded(wug[:, cols]) * fcol * upsc[0:1, cols]).astype(BF)
        g_up[j, z, y, :, 128:256] = (rounded(wuv[:, cols]) * fcol * upsc[1:2, cols]).astype(BF)
    tail = slice(640, 704)
    g_ul[0, z, y] = (
        jnp.concatenate(
            [rounded(wug[:, tail]) * upsc[0:1, tail], rounded(wuv[:, tail]) * upsc[1:2, tail]], axis=1
        )
        * fcol
    ).astype(BF)
    for k in range(2):
        g_dn[k, z, y] = (rounded(wd[256 * k : 256 * k + 256, :]) * dsc[...]).astype(BF)
    g_dl[0, z, y] = (rounded(wd[512:704, :]) * dsc[...]).astype(BF)

    pl.semaphore_wait(barrier, 7)

    rounds = (
        [(g_in, k, 128) for k in range(3)]
        + [(g_mo, 0, 256)]
        + [(g_up, k, 128) for k in range(5)]
        + [(g_ul, 0, 128)]
        + [(g_dn, k, 256) for k in range(2)]
        + [(g_dl, 0, 192)]
    )

    def block(r, h, p_at, q_at, lo, n):
        ref, k, rows = rounds[r]
        zz, yy = (q_at, p_at) if h == 0 else (p_at, q_at)
        return ref.at[k, zz, yy, pl.ds(lo, n), :]

    def line(r, h, q_at, lo, n):
        ref, k, rows = rounds[r]
        if h == 0:
            return ref.at[k, q_at, pl.ds(0, 4), pl.ds(lo, n), :]
        return ref.at[k, pl.ds(0, 4), q_at, pl.ds(lo, n), :]

    def geometry(r, h):
        half = rounds[r][2] // 2
        lo = half * h
        return lo, half, lo, lo + half // 2, half // 2, pos[h], pos[1 - h]

    def s1(r):
        if not 0 <= r < ROUNDS:
            return
        for h in range(2):
            lo, half, up, dn, quarter, p, q = geometry(r, h)
            own = block(r, h, p, q, lo, half)
            for d in range(2):
                send(own, own, y_send.at[r, h, d], y_recv.at[r, h, d], dev_axis[h][d])

    def s2(r):
        if not 0 <= r < ROUNDS:
            return
        for h in range(2):
            lo, half, up, dn, quarter, p, q = geometry(r, h)
            for d, at, part in ((0, (p + 3) % 4, up), (1, (p + 1) % 4, dn)):
                arrived(block(r, h, at, q, lo, half), y_recv.at[r, h, d])
                piece = block(r, h, at, q, part, quarter)
                send(piece, piece, y_send.at[r, h, 2 + d], y_recv.at[r, h, 2 + d], dev_axis[h][d])

    def s3(r):
        if not 0 <= r < ROUNDS:
            return
        for h in range(2):
            lo, half, up, dn, quarter, p, q = geometry(r, h)
            for d, part in ((0, up), (1, dn)):
                arrived(block(r, h, (p + 2) % 4, q, part, quarter), y_recv.at[r, h, 2 + d])
            row = line(r, h, q, lo, half)
            for d in range(2):
                send(row, row, y_send.at[r, h, 4 + d], y_recv.at[r, h, 4 + d], dev_axis[1 - h][d])

    def s4(r):
        if not 0 <= r < ROUNDS:
            return
        for h in range(2):
            lo, half, up, dn, quarter, p, q = geometry(r, h)
            for d, at, part in ((0, (q + 3) % 4, up), (1, (q + 1) % 4, dn)):
                arrived(line(r, h, at, lo, half), y_recv.at[r, h, 4 + d])
                piece = line(r, h, at, part, quarter)
                send(piece, piece, y_send.at[r, h, 6 + d], y_recv.at[r, h, 6 + d], dev_axis[1 - h][d])

    def done(r):
        for h in range(2):
            lo, half, up, dn, quarter, p, q = geometry(r, h)
            for d, part in ((0, up), (1, dn)):
                arrived(line(r, h, (q + 2) % 4, part, quarter), y_recv.at[r, h, 6 + d])

    def tick(k):
        s1(k + 2)
        s2(k + 1)
        s3(k)
        s4(k - 1)

    def cols_of(xx, cc):
        return pl.ds(pl.multiple_of((xx * 2 + cc) * W, W), W)

    def gather_own(u, buf, s, src):
        dst = buf.at[s, :, cols_of(x, core)]
        send(src, dst, a_send.at[u, 0], a_recv.at[u, 0], dev_xp)
        send(src, dst, a_send.at[u, 1], a_recv.at[u, 1], dev_xm)
        send(src, dst, a_send.at[u, 2], a_recv.at[u, 4], dev_sib)

    def gather_near(u, buf, s):
        for d, xx, lo, dev in ((0, xm, 0, dev_xp), (1, xp, HALF, dev_xm)):
            whole = buf.at[s, :, cols_of(xx, core)]
            arrived(whole, a_recv.at[u, d])
            piece = buf.at[s, pl.ds(lo, HALF), cols_of(xx, core)]
            send(piece, piece, a_send.at[u, 3 + d], a_recv.at[u, 2 + d], dev)
            send(whole, whole, a_send.at[u, 5 + d], a_recv.at[u, 5 + d], dev_sib)

    def gather_far(u, buf, s):
        for d, lo in ((0, 0), (1, HALF)):
            arrived(buf.at[s, pl.ds(lo, HALF), cols_of(xf, core)], a_recv.at[u, 2 + d])
        whole = buf.at[s, :, cols_of(xf, core)]
        send(whole, whole, a_send.at[u, 7], a_recv.at[u, 7], dev_sib)

    def gather_done(u, buf, s):
        for k, xx in ((4, x), (5, xm), (6, xp), (7, xf)):
            arrived(buf.at[s, :, cols_of(xx, 1 - core)], a_recv.at[u, k])

    def row_factor(buf, fac, s):
        total = jnp.zeros((SEQ, 128), F32)
        for j in range(D // 128):
            v = buf[s, :, 128 * j : 128 * j + 128].astype(F32)
            total = total + v * v
        mean = jnp.sum(total, axis=1, keepdims=True) * (1.0 / D)
        fac[s] = jnp.broadcast_to(lax.rsqrt(mean + EPS), (SEQ, 128))

    def shifted(v, n):
        row = lax.broadcasted_iota(jnp.int32, v.shape, 0)
        return jnp.where(row >= n, pltpu.roll(v, n, 0), 0.0)

    def causal(v, taps):
        return shifted(v, 2) * taps[0:1] + shifted(v, 1) * taps[1:2] + v * taps[2:3]

    def wide(fac, s):
        f = fac[s]
        return jnp.concatenate([f, f], axis=1)

    order = (xf, xp, xm, x)

    def scatter_parts(u, part):
        for k, xx in enumerate(order):
            sb[u, k] = part(xx, 1 - core).astype(BF)
            send(sb.at[u, k], rb.at[u, k], r_send.at[u, k], r_recv.at[u, k], dev_sib)
            keep[u, k] = part(xx, core)

    def scatter_far(u):
        arrived(rb.at[u, 0], r_recv.at[u, 0])
        fbuf[u] = (keep[u, 0] + rb[u, 0].astype(F32)).astype(BF)
        for d, dev in ((0, dev_xp), (1, dev_xm)):
            send(
                fbuf.at[u, pl.ds(HALF * d, HALF)], rf.at[u, d],
                r_send.at[u, 4 + d], r_recv.at[u, 4 + d], dev,
            )

    def scatter_near(u):
        for d, dev in ((0, dev_xp), (1, dev_xm)):
            arrived(rb.at[u, 1 + d], r_recv.at[u, 1 + d])
            lo = HALF * (1 - d)
            nbuf[u, d, lo : lo + HALF] = (
                keep[u, 1 + d, lo : lo + HALF] + rb[u, 1 + d, lo : lo + HALF].astype(F32)
            ).astype(BF)
            rows = pl.ds(lo, HALF)
            send(nbuf.at[u, d, rows], rn.at[u, d, rows], r_send.at[u, 6 + d], r_recv.at[u, 6 + d], dev)

    def scatter_last(u):
        for d, dev in ((0, dev_xp), (1, dev_xm)):
            arrived(rf.at[u, d], r_recv.at[u, 4 + d])
            lo = HALF * d
            nbuf[u, d, lo : lo + HALF] = (
                keep[u, 1 + d, lo : lo + HALF]
                + rb[u, 1 + d, lo : lo + HALF].astype(F32)
                + rf[u, d].astype(F32)
            ).astype(BF)
            rows = pl.ds(lo, HALF)
            send(nbuf.at[u, d, rows], rn.at[u, d, rows], r_send.at[u, 8 + d], r_recv.at[u, 8 + d], dev)

    def scatter_total(u):
        arrived(rb.at[u, 3], r_recv.at[u, 3])
        for d in range(2):
            for k, lo in ((6, HALF * (1 - d)), (8, HALF * d)):
                arrived(rn.at[u, d, pl.ds(lo, HALF)], r_recv.at[u, k + d])
        return keep[u, 3] + rb[u, 3].astype(F32) + rn[u, 0].astype(F32) + rn[u, 1].astype(F32)

    def dot(a, b):
        return jnp.dot(a, b, preferred_element_type=F32)

    def in_cgate():
        @pl.loop(0, 2)
        def _(s):
            cbuf[s] = dot(tfull[s], g_in[0].reshape(D, W))

    def in_value():
        @pl.loop(0, 2)
        def _(s):
            f = wide(tfac, s)
            inner = dot(tfull[s], g_in[1].reshape(D, W)) * cbuf[s] * (f * f)
            cbuf[s] = causal(inner, mtaps) * f

    def in_bgate():
        @pl.loop(0, 2)
        def _(s):
            gated[s] = (dot(tfull[s], g_in[2].reshape(D, W)) * cbuf[s]).astype(BF)

    def mix_part(s):
        def part(xx, cc):
            mat = jnp.concatenate([g_mo[0, xx, 2 * cc], g_mo[0, xx, 2 * cc + 1]], axis=1)
            return dot(gated[s], mat)

        return part

    def up(s):
        @pl.loop(0, 5)
        def _(j):
            cols = pl.ds(pl.multiple_of(128 * j, 128), 128)
            pre = dot(rfull[s], g_up[j].reshape(D, W)) * wide(rfac, s)
            taps = jnp.concatenate([ftaps[0, :, cols], ftaps[1, :, cols]], axis=1)
            conv = causal(pre, taps)
            gate, val = conv[:, 0:128], conv[:, 128:256]
            active[s, :, cols] = (gate / (1.0 + jnp.exp(-gate)) * val).astype(BF)

        pre = dot(rfull[s], g_ul[0].reshape(D, 128)) * rfac[s]
        taps = jnp.concatenate([ftaps[0, :, tail], ftaps[1, :, tail]], axis=1)
        conv = causal(pre, taps)
        act = conv / (1.0 + jnp.exp(-conv)) * pltpu.roll(conv, 64, 1)
        active[s, :, 640:704] = act[:, 0:64].astype(BF)

    def down_part(s):
        def part(xx, cc):
            total = None
            for ref, k, lo, n in ((g_dn, 0, 0, 256), (g_dn, 1, 256, 256), (g_dl, 0, 512, 192)):
                mat = jnp.concatenate([ref[k, xx, 2 * cc], ref[k, xx, 2 * cc + 1]], axis=1)
                term = dot(active[s, :, lo : lo + n], mat)
                total = term if total is None else total + term
            return total

        return part

    own = cols_of(x, core)

    s1(0)
    for s in range(2):
        gather_own(s, tfull, s, tok.at[s])
    s1(1)
    for s in range(2):
        tfull[s, :, own] = tok[s]
    s2(0)
    tick(0)
    gather_near(0, tfull, 0)
    tick(1)
    gather_near(1, tfull, 1)
    gather_far(0, tfull, 0)
    tick(2)
    gather_far(1, tfull, 1)
    for s in range(2):
        gather_done(s, tfull, s)
        row_factor(tfull, tfac, s)
    done(0)
    in_cgate()
    tick(3)
    done(1)
    in_value()
    tick(4)
    done(2)
    in_bgate()
    tick(5)
    done(3)
    scatter_parts(0, mix_part(0))
    scatter_far(0)
    scatter_near(0)
    scatter_parts(1, mix_part(1))
    scatter_far(1)
    scatter_near(1)
    tick(6)
    scatter_last(0)
    scatter_last(1)
    tick(7)

    def residual(s):
        rfull[s, :, own] = (tok[s].astype(F32) + scatter_total(s)).astype(BF)
        gather_own(2 + s, rfull, s, rfull.at[s, :, own])

    residual(0)
    tick(8)
    residual(1)
    tick(9)
    gather_near(2, rfull, 0)
    gather_near(3, rfull, 1)
    tick(10)
    gather_far(2, rfull, 0)
    gather_far(3, rfull, 1)
    tick(11)
    for r in range(4, 10):
        done(r)
    for s in range(2):
        gather_done(2 + s, rfull, s)
        row_factor(rfull, rfac, s)
        up(s)
        if s == 0:
            tick(12)
            tick(13)
    for r in range(10, 13):
        done(r)
    for s in range(2):
        scatter_parts(2 + s, down_part(s))
        scatter_far(2 + s)
        scatter_near(2 + s)
    for s in range(2):
        scatter_last(2 + s)
    for s in range(2):
        out[s] = (rfull[s, :, own].astype(F32) + scatter_total(2 + s)).astype(BF)
    for copy in started:
        copy.wait_send()


def on_device(
    tokens, mix_gain, w_bgate, w_cgate, w_value, in_scale, mix_taps, w_mixout, mixout_scale,
    ffn_gain, w_upgate, w_upval, up_scale, ffn_taps, w_down, down_scale,
):
    args = (
        tokens, mix_gain.reshape(16, 128), w_bgate, w_cgate, w_value, in_scale, mix_taps, w_mixout,
        mixout_scale, ffn_gain.reshape(16, 128), w_upgate, w_upval, up_scale, ffn_taps, w_down, down_scale,
    )
    vmem = pltpu.VMEM
    dma = pltpu.SemaphoreType.DMA
    return pl.pallas_call(
        kernel,
        out_shape=jax.ShapeDtypeStruct(tokens.shape, BF),
        in_specs=[pl.BlockSpec(memory_space=pltpu.VMEM)] * len(args),
        out_specs=pl.BlockSpec(memory_space=pltpu.VMEM),
        scratch_shapes=[
            vmem((3, 4, 4, 128, W), BF),
            vmem((1, 4, 4, 256, 128), BF),
            vmem((5, 4, 4, 128, W), BF),
            vmem((1, 4, 4, 128, 128), BF),
            vmem((2, 4, 4, 256, 128), BF),
            vmem((1, 4, 4, 192, 128), BF),
            vmem((2, SEQ, D), BF),
            vmem((2, SEQ, D), BF),
            vmem((2, SEQ, W), F32),
            vmem((2, SEQ, W), BF),
            vmem((2, SEQ, 704), BF),
            vmem((2, SEQ, 128), F32),
            vmem((2, SEQ, 128), F32),
            vmem((4, 4, SEQ, W), BF),
            vmem((4, 4, SEQ, W), BF),
            vmem((4, 4, SEQ, W), F32),
            vmem((4, SEQ, W), BF),
            vmem((4, 2, SEQ, W), BF),
            vmem((4, 2, HALF, W), BF),
            vmem((4, 2, SEQ, W), BF),
            dma((ROUNDS, 2, 8)),
            dma((ROUNDS, 2, 8)),
            dma((4, 8)),
            dma((4, 8)),
            dma((4, 10)),
            dma((4, 10)),
        ],
        compiler_params=pltpu.CompilerParams(
            collective_id=0, has_side_effects=True, vmem_limit_bytes=62 * 1024 * 1024
        ),
        name="layer",
    )(*args)


def solution(mesh):
    return jax.shard_map(
        on_device,
        mesh=mesh,
        in_specs=(
            P("fs", None, "tp"),
            P(),
            P("fs", "tp"),
            P("fs", "tp"),
            P("fs", "tp"),
            P(None, "tp"),
            P(None, "tp"),
            P("tp", "fs"),
            P(None, "fs"),
            P(),
            P("fs", "tp"),
            P("fs", "tp"),
            P(None, "tp"),
            P(None, None, "tp"),
            P("tp", "fs"),
            P(None, "fs"),
        ),
        out_specs=P("fs", None, "tp"),
        check_vma=False,
    )
```

time: 237 us -> 117 us (0.49)
  Pallas kernels: 0 us -> 111 us
  blocking collectives: 79.8 us -> 0 us
  waiting for transfers between devices: 55.6 us -> 0 us
  local copies, waits for them, and re-layouts: 28.5 us -> 5.95 us
  matrix products: 20.7 us -> 0 us
  other arithmetic: 19.7 us -> 0 us
  starting transfers between devices: 18.4 us -> 0 us
  between operations: 13.6 us -> 0.01 us
    pallas_call x0 -> x1, Pallas kernels: none -> 111 us  [on_device(): pl.pallas_call(kernel, out_shape=jax.ShapeDtypeStruct(tokens.shape, BF),...]
    all_to_all x3 -> x0, blocking collectives: 58.9 us -> none  [the longest x1 40.2 us: sum_at_owner(): parts = lax.all_to_all(split_up(value, dim, peers), axis, 0, 0, tiled=True)]
    all_to_all x4 -> x0, waiting for transfers between devices: 55.4 us -> none  [the longest x1 35.7 us: sum_at_owner(): parts = lax.all_to_all(split_up(value, dim, peers), axis, 0, 0, tiled=True)]
    all_gather x1 -> x0, blocking collectives: 20.8 us -> none  [in_one_piece(): out = lax.all_gather(both, axis, axis=dim, tiled=True)]
    dot_general x7 -> x0, matrix products: 20.7 us -> none  [the longest x5 13.5 us: dot_rows(): return jnp.dot(inputs, matrix, preferred_element_type=jnp.float32)]
    all_to_all x4 -> x0, starting transfers between devices: 18.4 us -> none  [the longest x3 12.9 us: copy_for_each(): lax.all_to_all(jnp.broadcast_to(value[None], (peers, *value.shape)), axis...]
    convert_element_type x13 -> x0, other arithmetic: 12.7 us -> none  [the longest x1 3.61 us: normed_rows(): result = (floats * factor * gain).astype(jnp.bfloat16)]
    convert_element_type x3 -> x0, local copies, waits for them, and re-layouts: 8.02 us -> none  [the longest x2 7.29 us: normed_rows(): floats = gathered.astype(jnp.float32)]
  transfers between devices with their start and end apart: 7 -> 0, of which waited for: 2 -> 0; matrix products, arithmetic and copies ran while one was open for 25% -> 0% of each run, Pallas kernels for 0% -> 0%
where the time goes in v1:
time: 117 us
  Pallas kernels  111 us (95%)
  local copies, waits for them, and re-layouts  5.95 us (5%)
    pallas_call x1, Pallas kernels, on_device(): pl.pallas_call(kernel, out_shape=jax.ShapeDtypeStruct(tokens.shape, BF),...  111 us
    unnamed x6, local copies, waits for them, and re-layouts  5.95 us

profile of v1, /device:TPU:1, one launch (start us, length us, event | category | flops | bytes accessed | tf_op | source)
XLA Modules:
  0.0 117.1 jit_solution(5243099722809878883)
XLA Ops:
  0.0 1.3 %copy.19.ftaps = f32[2,3,704]{2,1,0:T(4,128)} copy(f32[2,3,704]{2,0,1:T(2,128)} %param.29) | data formatting | bytes 33792 | tf_op args[13]
  1.3 0.0 copy-start
  1.3 1.9 %copy.17.wug = f32[128,704]{1,0:T(8,128)} copy(f32[128,704]{0,1:T(8,128)} %param.26) | data formatting | bytes 720896 | tf_op args[10]
  3.3 0.0 copy-done
  3.3 0.9 copy.18.wuv
  4.2 111.1 %layer.1 = bf16[2,384,256]{2,1,0:T(8,128)(2,1)} custom-call(bf16[2,384,256]{2,1,0:T(8,128)(2,1)} %tok.1, f32[16,128]{1,0:T(8,128)} %bitcast.2, f32[128,256]{1,0:T(8,128)} %wb.1, f32[128,256]{1,0:T(8,128)} %wc.1, f32[128,256]{1,0:T(8,128)} %wv.1, f32[3,256]{1,0:T(4,128)} %insc.1, f32[3,256]{1,0:T(4,128)} %mtaps.1, f32[256,128]{1,0:T(8,128)} %wm.1, ...), custom_call_target="tpu_custom_call" | custom-call | tf_op jit(solution)/shard_map/layer/pallas_call | solution.py:397
  115.3 1.8 %copy.21 = bf16[2,384,256]{2,1,0:T(8,128)(2,1)} copy(bf16[2,384,256]{2,1,0:T(8,128)(2,1)} %layer.1) | data formatting | bytes 786432
Async XLA Ops:
  1.3 2.0 %copy-start = (f32[128,704]{0,1:T(8,128)S(1)}, f32[128,704]{0,1:T(8,128)}, u32[]{:S(2)}) copy-start(f32[128,704]{0,1:T(8,128)} %param.27) | copy-start | bytes 1081348

commit v2 on v1

--- a/solution.py
+++ b/solution.py
@@ -38,15 +38,17 @@
         ((((z + 1) % 4) * 4 + y, tp), (((z + 3) % 4) * 4 + y, tp)),
     )
     pos = (y, z)
-    started = []
-
-    def send(src, dst, ssem, rsem, dev):
-        copy = pltpu.make_async_remote_copy(
+    sent = []
+
+    def push(src, dst, ssem, rsem, dev):
+        pltpu.make_async_remote_copy(
             src_ref=src, dst_ref=dst, send_sem=ssem, recv_sem=rsem,
             device_id=dev, device_id_type=pl.DeviceIdType.MESH,
-        )
-        copy.start()
-        started.append(copy)
+        ).start()
+
+    def send(src, dst, ssem, rsem, dev):
+        push(src, dst, ssem, rsem, dev)
+        sent.append((src, ssem))
 
     def arrived(dst, rsem):
         pltpu.make_async_copy(dst, dst, rsem).wait()
@@ -66,18 +68,17 @@
     for k, (w, row) in enumerate(((wc, 1), (wv, 2), (wb, 0))):
         g_in[k, z, y] = (rounded(w[...]) * mcol2 * insc[row : row + 1, :]).astype(BF)
     g_mo[0, z, y] = (rounded(wm[...]) * msc[...]).astype(BF)
-    fcol = column(fgain)
+    frow = fgain[pl.ds(fs, 1), :]
     for j in range(5):
         cols = slice(128 * j, 128 * j + 128)
-        g_up[j, z, y, :, 0:128] = (rounded(wug[:, cols]) * fcol * upsc[0:1, cols]).astype(BF)
-        g_up[j, z, y, :, 128:256] = (rounded(wuv[:, cols]) * fcol * upsc[1:2, cols]).astype(BF)
+        for k, w in enumerate((wug, wuv)):
+            g_up[j, z, y, :, 128 * k : 128 * k + 128] = (
+                (rounded(w[cols, :]) * frow).T * upsc[k : k + 1, cols]
+            ).astype(BF)
     tail = slice(640, 704)
-    g_ul[0, z, y] = (
-        jnp.concatenate(
-            [rounded(wug[:, tail]) * upsc[0:1, tail], rounded(wuv[:, tail]) * upsc[1:2, tail]], axis=1
-        )
-        * fcol
-    ).astype(BF)
+    both = rounded(jnp.concatenate([wug[tail, :], wuv[tail, :]], axis=0))
+    tail_scale = jnp.concatenate([upsc[0:1, tail], upsc[1:2, tail]], axis=1)
+    g_ul[0, z, y] = ((both * frow).T * tail_scale).astype(BF)
     for k in range(2):
         g_dn[k, z, y] = (rounded(wd[256 * k : 256 * k + 256, :]) * dsc[...]).astype(BF)
     g_dl[0, z, y] = (rounded(wd[512:704, :]) * dsc[...]).astype(BF)
@@ -117,6 +118,13 @@
             own = block(r, h, p, q, lo, half)
             for d in range(2):
                 send(own, own, y_send.at[r, h, d], y_recv.at[r, h, d], dev_axis[h][d])
+            across(r, h, p)
+
+    def across(r, h, p_at):
+        lo, half, up, dn, quarter, p, q = geometry(r, h)
+        piece = block(r, h, p_at, q, lo, half)
+        for d in range(2):
+            push(piece, piece, y_send.at[r, h, 4 + d], y_recv.at[r, h, 4 + d], dev_axis[1 - h][d])
 
     def s2(r):
         if not 0 <= r < ROUNDS:
@@ -127,6 +135,7 @@
                 arrived(block(r, h, at, q, lo, half), y_recv.at[r, h, d])
                 piece = block(r, h, at, q, part, quarter)
                 send(piece, piece, y_send.at[r, h, 2 + d], y_recv.at[r, h, 2 + d], dev_axis[h][d])
+                across(r, h, at)
 
     def s3(r):
         if not 0 <= r < ROUNDS:
@@ -135,9 +144,9 @@
             lo, half, up, dn, quarter, p, q = geometry(r, h)
             for d, part in ((0, up), (1, dn)):
                 arrived(block(r, h, (p + 2) % 4, q, part, quarter), y_recv.at[r, h, 2 + d])
-            row = line(r, h, q, lo, half)
+            across(r, h, (p + 2) % 4)
             for d in range(2):
-                send(row, row, y_send.at[r, h, 4 + d], y_recv.at[r, h, 4 + d], dev_axis[1 - h][d])
+                sent.append((line(r, h, q, lo, half), y_send.at[r, h, 4 + d]))
 
     def s4(r):
         if not 0 <= r < ROUNDS:
@@ -146,8 +155,10 @@
             lo, half, up, dn, quarter, p, q = geometry(r, h)
             for d, at, part in ((0, (q + 3) % 4, up), (1, (q + 1) % 4, dn)):
                 arrived(line(r, h, at, lo, half), y_recv.at[r, h, 4 + d])
-                piece = line(r, h, at, part, quarter)
-                send(piece, piece, y_send.at[r, h, 6 + d], y_recv.at[r, h, 6 + d], dev_axis[1 - h][d])
+                for k in range(4):
+                    piece = block(r, h, k, at, part, quarter)
+                    push(piece, piece, y_send.at[r, h, 6 + d], y_recv.at[r, h, 6 + d], dev_axis[1 - h][d])
+                sent.append((line(r, h, at, part, quarter), y_send.at[r, h, 6 + d]))
 
     def done(r):
         for h in range(2):
@@ -285,13 +296,13 @@
         def _(j):
             cols = pl.ds(pl.multiple_of(128 * j, 128), 128)
             pre = dot(rfull[s], g_up[j].reshape(D, W)) * wide(rfac, s)
-            taps = jnp.concatenate([ftaps[0, :, cols], ftaps[1, :, cols]], axis=1)
+            taps = jnp.concatenate([ftaps[:, 0, cols], ftaps[:, 1, cols]], axis=1)
             conv = causal(pre, taps)
             gate, val = conv[:, 0:128], conv[:, 128:256]
             active[s, :, cols] = (gate / (1.0 + jnp.exp(-gate)) * val).astype(BF)
 
         pre = dot(rfull[s], g_ul[0].reshape(D, 128)) * rfac[s]
-        taps = jnp.concatenate([ftaps[0, :, tail], ftaps[1, :, tail]], axis=1)
+        taps = jnp.concatenate([ftaps[:, 0, tail], ftaps[:, 1, tail]], axis=1)
         conv = causal(pre, taps)
         act = conv / (1.0 + jnp.exp(-conv)) * pltpu.roll(conv, 64, 1)
         active[s, :, 640:704] = act[:, 0:64].astype(BF)
@@ -341,9 +352,9 @@
     scatter_near(0)
     scatter_parts(1, mix_part(1))
     scatter_far(1)
-    scatter_near(1)
     tick(6)
     scatter_last(0)
+    scatter_near(1)
     scatter_last(1)
     tick(7)
 
@@ -354,8 +365,8 @@
     residual(0)
     tick(8)
     residual(1)
+    gather_near(2, rfull, 0)
     tick(9)
-    gather_near(2, rfull, 0)
     gather_near(3, rfull, 1)
     tick(10)
     gather_far(2, rfull, 0)
@@ -372,16 +383,18 @@
             tick(13)
     for r in range(10, 13):
         done(r)
-    for s in range(2):
-        scatter_parts(2 + s, down_part(s))
-        scatter_far(2 + s)
-        scatter_near(2 + s)
-    for s in range(2):
-        scatter_last(2 + s)
+    scatter_parts(2, down_part(0))
+    scatter_far(2)
+    scatter_near(2)
+    scatter_parts(3, down_part(1))
+    scatter_far(3)
+    scatter_last(2)
+    scatter_near(3)
+    scatter_last(3)
     for s in range(2):
         out[s] = (rfull[s, :, own].astype(F32) + scatter_total(2 + s)).astype(BF)
-    for copy in started:
-        copy.wait_send()
+    for src, ssem in sent:
+        arrived(src, ssem)
 
 
 def on_device(
@@ -390,7 +403,8 @@
 ):
     args = (
         tokens, mix_gain.reshape(16, 128), w_bgate, w_cgate, w_value, in_scale, mix_taps, w_mixout,
-        mixout_scale, ffn_gain.reshape(16, 128), w_upgate, w_upval, up_scale, ffn_taps, w_down, down_scale,
+        mixout_scale, ffn_gain.reshape(16, 128), w_upgate.T, w_upval.T, up_scale,
+        jnp.swapaxes(ffn_taps, 0, 1), w_down, down_scale,
     )
     vmem = pltpu.VMEM
     dma = pltpu.SemaphoreType.DMA

time: 117 us -> 112 us (0.957)
  local copies, waits for them, and re-layouts: 5.95 us -> 1.77 us
    unnamed x6 -> x1, local copies, waits for them, and re-layouts: 5.95 us -> 1.77 us
where the time goes in v2:
time: 112 us
  Pallas kernels  110 us (98%)
  local copies, waits for them, and re-layouts  1.77 us (2%)
    pallas_call x1, Pallas kernels, on_device(): pl.pallas_call(kernel, out_shape=jax.ShapeDtypeStruct(tokens.shape, BF),...  110 us

profile of v2, /device:TPU:1, one launch (start us, length us, event | category | flops | bytes accessed | tf_op | source)
XLA Modules:
  0.0 111.9 jit_solution(10671313141623020605)
XLA Ops:
  0.0 110.1 %layer.1 = bf16[2,384,256]{2,1,0:T(8,128)(2,1)} custom-call(bf16[2,384,256]{2,1,0:T(8,128)(2,1)} %tok.1, f32[16,128]{1,0:T(8,128)} %bitcast.8, f32[128,256]{1,0:T(8,128)} %wb.1, f32[128,256]{1,0:T(8,128)} %wc.1, f32[128,256]{1,0:T(8,128)} %wv.1, f32[3,256]{1,0:T(4,128)} %insc.1, f32[3,256]{1,0:T(4,128)} %mtaps.1, f32[256,128]{1,0:T(8,128)} %wm.1, ...), custom_call_target="tpu_custom_call" | custom-call | tf_op jit(solution)/shard_map/layer/pallas_call | solution.py:411
  110.2 1.8 %copy.18 = bf16[2,384,256]{2,1,0:T(8,128)(2,1)} copy(bf16[2,384,256]{2,1,0:T(8,128)(2,1)} %layer.1) | data formatting | bytes 786432

commit v3 on v2

v3 whole, which is shorter than its diff:
```python
import functools

import jax
import jax.numpy as jnp
from jax import lax
from jax.experimental import pallas as pl
from jax.experimental.pallas import tpu as pltpu
from jax.sharding import PartitionSpec as P

EPS = 1e-06
BF = jnp.bfloat16
F32 = jnp.float32
SEQ = 384
HALF = SEQ // 2
D = 2048
W = 256
ROUNDS = 13


def kernel(
    tok_h, mgain_h, wb_h, wc_h, wv_h, insc_h, mtaps_h, wm_h, msc_h, fgain_h, wug_h, wuv_h, upsc_h, ftaps_h,
    wd_h, dsc_h,
    out,
    mgain, wb, wc, wv, insc, mtaps, wm, msc, fgain, wug, wuv, upsc, ftaps, wd, dsc,
    g_in, g_mo, g_up, g_ul, g_dt, g_d,
    tfull, rfull, cbuf, gated, active, fac, squares, acc, acc_tail,
    sb, rb, keep, fbuf, nbuf, rf, rn,
    sb2, rb2, keep2, fbuf2, nbuf2, rf2, rn2,
    y_send, y_recv, a_send, a_recv, r_send, r_recv, load_sem,
):
    fs = lax.axis_index("fs")
    tp = lax.axis_index("tp")
    z, y = fs // 4, fs % 4
    x, core = tp // 2, tp % 2
    xp, xm, xf = (x + 1) % 4, (x + 3) % 4, (x + 2) % 4
    dev_xp = (fs, xp * 2 + core)
    dev_xm = (fs, xm * 2 + core)
    dev_sib = (fs, x * 2 + 1 - core)
    dev_axis = (
        ((z * 4 + (y + 1) % 4, tp), (z * 4 + (y + 3) % 4, tp)),
        ((((z + 1) % 4) * 4 + y, tp), (((z + 3) % 4) * 4 + y, tp)),
    )
    pos = (y, z)
    sent = []

    def push(src, dst, ssem, rsem, dev):
        pltpu.make_async_remote_copy(
            src_ref=src, dst_ref=dst, send_sem=ssem, recv_sem=rsem,
            device_id=dev, device_id_type=pl.DeviceIdType.MESH,
        ).start()

    def send(src, dst, ssem, rsem, dev):
        push(src, dst, ssem, rsem, dev)
        sent.append((src, ssem))

    def arrived(dst, rsem):
        pltpu.make_async_copy(dst, dst, rsem).wait()

    barrier = pltpu.get_barrier_semaphore()
    for dev in (*dev_axis[0], *dev_axis[1], dev_xp, dev_xm, dev_sib):
        pl.semaphore_signal(barrier, inc=1, device_id=dev, device_id_type=pl.DeviceIdType.MESH)

    loads = {}

    def load(name, src, dst):
        loads[name] = pltpu.make_async_copy(src, dst, load_sem.at[len(loads)])
        loads[name].start()

    def cols_of(xx, cc):
        return pl.ds(pl.multiple_of((xx * 2 + cc) * W, W), W)

    for s in range(2):
        load(("tok", s), tok_h.at[s], tfull.at[s, :, cols_of(x, core)])
    for name, src, dst in (
        ("mgain", mgain_h, mgain), ("insc", insc_h, insc), ("wc", wc_h, wc), ("wv", wv_h, wv), ("wb", wb_h, wb),
        ("msc", msc_h, msc), ("wm", wm_h, wm), ("fgain", fgain_h, fgain), ("upsc", upsc_h, upsc),
        ("wug", wug_h, wug), ("wuv", wuv_h, wuv), ("dsc", dsc_h, dsc), ("wd", wd_h, wd),
        ("mtaps", mtaps_h, mtaps), ("ftaps", ftaps_h, ftaps),
    ):
        load(name, src, dst)

    def ready(*names):
        for name in names:
            if name in loads:
                loads.pop(name).wait()

    def rounded(w):
        return w.astype(BF).astype(F32)

    tail = slice(640, 704)

    def pack(r):
        if r < 3:
            w, row = ((wc, 1), (wv, 2), (wb, 0))[r]
            ready("mgain", "insc", ("wc", "wv", "wb")[r])
            col = jnp.broadcast_to(mgain[pl.ds(fs, 1), :], (128, 128)).T
            col = jnp.concatenate([col, col], axis=1)
            g_in[r, z, y] = (rounded(w[...]) * col * insc[row : row + 1, :]).astype(BF)
        elif r == 3:
            ready("msc", "wm")
            g_mo[0, z, y] = (rounded(wm[...]) * msc[...]).astype(BF)
        elif r < 9:
            ready("fgain", "upsc", "wug", "wuv")
            frow = fgain[pl.ds(fs, 1), :]
            j = r - 4
            cols = slice(128 * j, 128 * j + 128)
            for k, w in enumerate((wug, wuv)):
                g_up[j, z, y, :, 128 * k : 128 * k + 128] = (
                    (rounded(w[cols, :]) * frow).T * upsc[k : k + 1, cols]
                ).astype(BF)
        elif r == 9:
            frow = fgain[pl.ds(fs, 1), :]
            both = rounded(jnp.concatenate([wug[tail, :], wuv[tail, :]], axis=0))
            tail_scale = jnp.concatenate([upsc[0:1, tail], upsc[1:2, tail]], axis=1)
            g_ul[0, z, y] = ((both * frow).T * tail_scale).astype(BF)
        elif r == 10:
            ready("dsc", "wd")
            last = rounded(wd[tail, :]) * dsc[...]
            turned = jnp.concatenate([last, last], axis=0).T
            lane = lax.broadcasted_iota(jnp.int32, (64, 128), 1)
            g_dt[0, z, y] = jnp.where(lane < 64, turned[0:64], turned[64:128]).astype(BF)
        elif r < 13:
            lo = 64 * (r - 11)
            for j in range(5):
                cols = slice(128 * j, 128 * j + 128)
                turned = (rounded(wd[cols, :]) * dsc[...]).T
                g_d[r - 11, z, y, :, cols] = turned[lo : lo + 64].astype(BF)

    rounds = (
        [(g_in, k, 128) for k in range(3)]
        + [(g_mo, 0, 256)]
        + [(g_up, k, 128) for k in range(5)]
        + [(g_ul, 0, 128), (g_dt, 0, 64)]
        + [(g_d, k, 64) for k in range(2)]
    )

    def block(r, h, p_at, q_at, lo, n):
        ref, k, rows = rounds[r]
        zz, yy = (q_at, p_at) if h == 0 else (p_at, q_at)
        return ref.at[k, zz, yy, pl.ds(lo, n), :]

    def line(r, h, q_at, lo, n):
        ref, k, rows = rounds[r]
        if h == 0:
            return ref.at[k, q_at, pl.ds(0, 4), pl.ds(lo, n), :]
        return ref.at[k, pl.ds(0, 4), q_at, pl.ds(lo, n), :]

    def geometry(r, h):
        half = rounds[r][2] // 2
        lo = half * h
        return lo, half, lo, lo + half // 2, half // 2, pos[h], pos[1 - h]

    def s1(r):
        if not 0 <= r < ROUNDS:
            return
        pack(r + 1)
        for h in range(2):
            lo, half, up, dn, quarter, p, q = geometry(r, h)
            own = block(r, h, p, q, lo, half)
            for d in range(2):
                send(own, own, y_send.at[r, h, d], y_recv.at[r, h, d], dev_axis[h][d])
            across(r, h, p)

    def across(r, h, p_at):
        lo, half, up, dn, quarter, p, q = geometry(r, h)
        piece = block(r, h, p_at, q, lo, half)
        for d in range(2):
            push(piece, piece, y_send.at[r, h, 4 + d], y_recv.at[r, h, 4 + d], dev_axis[1 - h][d])

    def s2(r):
        if not 0 <= r < ROUNDS:
            return
        for h in range(2):
            lo, half, up, dn, quarter, p, q = geometry(r, h)
            for d, at, part in ((0, (p + 3) % 4, up), (1, (p + 1) % 4, dn)):
                arrived(block(r, h, at, q, lo, half), y_recv.at[r, h, d])
                piece = block(r, h, at, q, part, quarter)
                send(piece, piece, y_send.at[r, h, 2 + d], y_recv.at[r, h, 2 + d], dev_axis[h][d])
                across(r, h, at)

    def s3(r):
        if not 0 <= r < ROUNDS:
            return
        for h in range(2):
            lo, half, up, dn, quarter, p, q = geometry(r, h)
            for d, part in ((0, up), (1, dn)):
                arrived(block(r, h, (p + 2) % 4, q, part, quarter), y_recv.at[r, h, 2 + d])
            across(r, h, (p + 2) % 4)
            for d in range(2):
                sent.append((line(r, h, q, lo, half), y_send.at[r, h, 4 + d]))

    def s4(r):
        if not 0 <= r < ROUNDS:
            return
        for h in range(2):
            lo, half, up, dn, quarter, p, q = geometry(r, h)
            for d, at, part in ((0, (q + 3) % 4, up), (1, (q + 1) % 4, dn)):
                arrived(line(r, h, at, lo, half), y_recv.at[r, h, 4 + d])
                for k in range(4):
                    piece = block(r, h, k, at, part, quarter)
                    push(piece, piece, y_send.at[r, h, 6 + d], y_recv.at[r, h, 6 + d], dev_axis[1 - h][d])
                sent.append((line(r, h, at, part, quarter), y_send.at[r, h, 6 + d]))

    def done(r):
        for h in range(2):
            lo, half, up, dn, quarter, p, q = geometry(r, h)
            for d, part in ((0, up), (1, dn)):
                arrived(line(r, h, (q + 2) % 4, part, quarter), y_recv.at[r, h, 6 + d])

    def ahead(k):
        s1(k + 2)
        s2(k + 1)
        s3(k)

    def tick(k):
        ahead(k)
        s4(k - 1)

    def gather_own(u, buf, s, src):
        dst = buf.at[s, :, cols_of(x, core)]
        send(src, dst, a_send.at[u, 0], a_recv.at[u, 0], dev_xp)
        send(src, dst, a_send.at[u, 1], a_recv.at[u, 1], dev_xm)
        send(src, dst, a_send.at[u, 2], a_recv.at[u, 4], dev_sib)

    def gather_near(u, buf, s):
        for d, xx, lo, dev in ((0, xm, 0, dev_xp), (1, xp, HALF, dev_xm)):
            whole = buf.at[s, :, cols_of(xx, core)]
            arrived(whole, a_recv.at[u, d])
            piece = buf.at[s, pl.ds(lo, HALF), cols_of(xx, core)]
            send(piece, piece, a_send.at[u, 3 + d], a_recv.at[u, 2 + d], dev)
            send(whole, whole, a_send.at[u, 5 + d], a_recv.at[u, 5 + d], dev_sib)

    def gather_far(u, buf, s):
        for d, lo in ((0, 0), (1, HALF)):
            arrived(buf.at[s, pl.ds(lo, HALF), cols_of(xf, core)], a_recv.at[u, 2 + d])
        whole = buf.at[s, :, cols_of(xf, core)]
        send(whole, whole, a_send.at[u, 7], a_recv.at[u, 7], dev_sib)

    def gather_done(u, buf, s):
        for k, xx in ((4, x), (5, xm), (6, xp), (7, xf)):
            arrived(buf.at[s, :, cols_of(xx, 1 - core)], a_recv.at[u, k])

    def wide_cols(xx):
        return pl.ds(pl.multiple_of(xx * 2 * W, 2 * W), 2 * W)

    def add_squares(buf, s, xx, first=False):
        v = buf[s, :, wide_cols(xx)].astype(F32)
        v = v * v
        total = v[:, 0:128] + v[:, 128:256] + v[:, 256:384] + v[:, 384:512]
        squares[s] = total if first else squares[s] + total

    def row_factor(s):
        mean = jnp.sum(squares[s], axis=1, keepdims=True) * (1.0 / D)
        fac[s] = jnp.broadcast_to(lax.rsqrt(mean + EPS), (SEQ, 128))

    def shifted(v, n):
        row = lax.broadcasted_iota(jnp.int32, v.shape, 0)
        return jnp.where(row >= n, pltpu.roll(v, n, 0), 0.0)

    def causal(v, taps):
        return shifted(v, 2) * taps[0:1] + shifted(v, 1) * taps[1:2] + v * taps[2:3]

    def wide(s):
        f = fac[s]
        return jnp.concatenate([f, f], axis=1)

    order = (xf, xp, xm, x)

    class Unit:
        def __init__(self, u, sems, sb, rb, keep, fbuf, nbuf, rf, rn):
            self.sb, self.rb, self.fbuf, self.nbuf, self.rf, self.rn = (
                ref.at[u] for ref in (sb, rb, fbuf, nbuf, rf, rn)
            )
            self.keep = keep
            self.ssem, self.rsem = r_send.at[sems], r_recv.at[sems]

        def part(self, k):
            send(self.sb.at[k], self.rb.at[k], self.ssem.at[k], self.rsem.at[k], dev_sib)

        def both(self, k, d):
            return self.keep(k, d) + self.rb[k, d].astype(F32)

        def far(self):
            arrived(self.rb.at[0], self.rsem.at[0])
            for d, dev in ((0, dev_xp), (1, dev_xm)):
                self.fbuf[d] = self.both(0, d).astype(BF)
            for d, dev in ((0, dev_xp), (1, dev_xm)):
                send(self.fbuf.at[d], self.rf.at[d], self.ssem.at[4 + d], self.rsem.at[4 + d], dev)

        def near(self):
            for d, dev in ((0, dev_xp), (1, dev_xm)):
                arrived(self.rb.at[1 + d], self.rsem.at[1 + d])
                self.nbuf[d, 1 - d] = self.both(1 + d, 1 - d).astype(BF)
            for d, dev in ((0, dev_xp), (1, dev_xm)):
                send(
                    self.nbuf.at[d, 1 - d], self.rn.at[d, 1 - d],
                    self.ssem.at[6 + d], self.rsem.at[6 + d], dev,
                )

        def last(self):
            for d, dev in ((0, dev_xp), (1, dev_xm)):
                arrived(self.rf.at[d], self.rsem.at[4 + d])
                self.nbuf[d, d] = (self.both(1 + d, d) + self.rf[d].astype(F32)).astype(BF)
                send(self.nbuf.at[d, d], self.rn.at[d, d], self.ssem.at[8 + d], self.rsem.at[8 + d], dev)

        def landed(self):
            arrived(self.rb.at[3], self.rsem.at[3])
            for d in range(2):
                arrived(self.rn.at[d, 1 - d], self.rsem.at[6 + d])
                arrived(self.rn.at[d, d], self.rsem.at[8 + d])

        def total(self, d):
            return self.both(3, d) + self.rn[0, d].astype(F32) + self.rn[1, d].astype(F32)

    def mix_unit(s):
        return Unit(s, s, sb, rb, lambda k, d: keep[s, k, d], fbuf, nbuf, rf, rn)

    def ffn_unit(h):
        return Unit(
            h, 2 + h, sb2, rb2, lambda k, d: keep2[h, k, 2 * core + d], fbuf2, nbuf2, rf2, rn2
        )

    def dot(a, b):
        return jnp.dot(a, b, preferred_element_type=F32)

    def in_cgate():
        @pl.loop(0, 2)
        def _(s):
            cbuf[s] = dot(tfull[s], g_in[0].reshape(D, W))

    def in_value():
        @pl.loop(0, 2)
        def _(s):
            f = wide(s)
            inner = dot(tfull[s], g_in[1].reshape(D, W)) * cbuf[s] * (f * f)
            cbuf[s] = causal(inner, mtaps) * f

    def in_bgate():
        @pl.loop(0, 2)
        def _(s):
            gated[s] = (dot(tfull[s], g_in[2].reshape(D, W)) * cbuf[s]).astype(BF)

    def mix_parts(s, unit):
        for k, xx in enumerate(order):
            for cc in (1 - core, core):
                mat = jnp.concatenate([g_mo[0, xx, 2 * cc], g_mo[0, xx, 2 * cc + 1]], axis=1)
                term = dot(gated[s], mat).reshape(2, HALF, W)
                if cc is core:
                    keep[s, k] = term
                else:
                    sb[s, k] = term.astype(BF)
                    unit.part(k)

    def up_dots(s, j, blocks):
        total = None
        for xx in blocks:
            mat = g_ul[0, xx].reshape(512, 128) if j is None else g_up[j, xx].reshape(512, W)
            term = dot(rfull[s, :, wide_cols(xx)], mat)
            total = term if total is None else total + term
        return total

    def up_first(s):
        @pl.loop(0, 5)
        def _(j):
            acc[s, j] = up_dots(s, j, (x, xm, xp))

        acc_tail[s] = up_dots(s, None, (x, xm, xp))

    def silu(v):
        return v / (1.0 + jnp.exp(-v))

    def up_second(s):
        @pl.loop(0, 5)
        def _(j):
            cols = pl.ds(pl.multiple_of(128 * j, 128), 128)
            pre = (acc[s, j] + up_dots(s, j, (xf,))) * wide(s)
            taps = jnp.concatenate([ftaps[:, 0, cols], ftaps[:, 1, cols]], axis=1)
            conv = causal(pre, taps)
            active[s, :, cols] = (silu(conv[:, 0:128]) * conv[:, 128:256]).astype(BF)

        pre = (acc_tail[s] + up_dots(s, None, (xf,))) * fac[s]
        taps = jnp.concatenate([ftaps[:, 0, tail], ftaps[:, 1, tail]], axis=1)
        conv = causal(pre, taps)
        act = silu(conv) * pltpu.roll(conv, 64, 1)
        lane = lax.broadcasted_iota(jnp.int32, (SEQ, 128), 1)
        act = jnp.where(lane < 64, act, 0.0)
        active[s, :, 640:768] = act.astype(BF)
        active[s, :, 768:896] = pltpu.roll(act, 64, 1).astype(BF)

    def turned_dot(a, b):
        return lax.dot_general(a, b, (((1,), (1,)), ((), ())), preferred_element_type=F32)

    def down_parts(h, unit):
        for k, xx in enumerate(order):
            for s in range(2):
                term = turned_dot(g_d[h, xx].reshape(256, 640), active[s, :, 0:640])
                lo = 640 + 128 * h
                term = term + turned_dot(g_dt[0, xx].reshape(256, 128), active[s, :, lo : lo + 128])
                keep2[h, k, :, :, SEQ * s : SEQ * s + SEQ] = term.reshape(4, 64, SEQ)
            sb2[h, k] = keep2[h, k, pl.ds(2 * (1 - core), 2)].astype(BF)
            unit.part(k)

    own = cols_of(x, core)

    ready(("tok", 0), ("tok", 1))
    pl.semaphore_wait(barrier, 7)
    for s in range(2):
        gather_own(s, tfull, s, tfull.at[s, :, own])
    pack(0)
    s1(0)
    s1(1)
    s2(0)
    tick(0)
    gather_near(0, tfull, 0)
    tick(1)
    gather_near(1, tfull, 1)
    gather_far(0, tfull, 0)
    tick(2)
    gather_far(1, tfull, 1)
    ready("mtaps", "ftaps")
    for s in range(2):
        gather_done(s, tfull, s)
        for xx in range(4):
            add_squares(tfull, s, xx, xx == 0)
        row_factor(s)
    ahead(3)
    done(0)
    in_cgate()
    s4(2)
    ahead(4)
    done(1)
    in_value()
    s4(3)
    done(2)
    in_bgate()
    ahead(5)
    done(3)
    u0, u1 = mix_unit(0), mix_unit(1)
    mix_parts(0, u0)
    u0.far()
    u0.near()
    s4(4)
    mix_parts(1, u1)
    u1.far()
    ahead(6)
    u0.last()
    u1.near()
    s4(5)
    u1.last()
    ahead(7)

    def residual(s, unit):
        unit.landed()
        for d in range(2):
            rows = slice(HALF * d, HALF * d + HALF)
            rfull[s, rows, own] = (tfull[s, rows, own].astype(F32) + unit.total(d)).astype(BF)
        gather_own(2 + s, rfull, s, rfull.at[s, :, own])

    residual(0, u0)
    s4(6)
    ahead(8)
    residual(1, u1)
    gather_near(2, rfull, 0)
    s4(7)
    ahead(9)
    for r in range(4, 8):
        done(r)
    gather_near(3, rfull, 1)
    tick(10)

    def near_done(u, buf, s):
        for k, xx in ((4, x), (5, xm), (6, xp)):
            arrived(buf.at[s, :, cols_of(xx, 1 - core)], a_recv.at[u, k])

    def far_done(u, buf, s):
        arrived(buf.at[s, :, cols_of(xf, 1 - core)], a_recv.at[u, 7])

    s4(8)
    tick(11)
    done(8)
    done(9)
    near_done(2, rfull, 0)
    for k, xx in enumerate((x, xm, xp)):
        add_squares(rfull, 0, xx, k == 0)
    up_first(0)
    gather_far(2, rfull, 0)
    tick(12)
    near_done(3, rfull, 1)
    for k, xx in enumerate((x, xm, xp)):
        add_squares(rfull, 1, xx, k == 0)
    up_first(1)
    gather_far(3, rfull, 1)
    tick(13)
    for s in range(2):
        far_done(2 + s, rfull, s)
        add_squares(rfull, s, xf)
        row_factor(s)
        up_second(s)
    done(10)
    done(11)
    v0, v1 = ffn_unit(0), ffn_unit(1)
    down_parts(0, v0)
    v0.far()
    v0.near()
    done(12)
    down_parts(1, v1)
    v1.far()
    v0.last()
    v1.near()
    v1.last()
    total = []
    for h, unit in enumerate((v0, v1)):
        unit.landed()
        total.append([unit.total(d) for d in range(2)])
    for s in range(2):
        for d in range(2):
            lanes = slice(SEQ * s, SEQ * s + SEQ)
            turned = jnp.concatenate([total[0][d][:, lanes], total[1][d][:, lanes]], axis=0).T
            cols = pl.ds(pl.multiple_of((x * 2 + core) * W + 128 * d, 128), 128)
            out[s, :, 128 * d : 128 * d + 128] = (rfull[s, :, cols].astype(F32) + turned).astype(BF)
    for src, ssem in sent:
        arrived(src, ssem)


def on_device(
    tokens, mix_gain, w_bgate, w_cgate, w_value, in_scale, mix_taps, w_mixout, mixout_scale,
    ffn_gain, w_upgate, w_upval, up_scale, ffn_taps, w_down, down_scale,
):
    args = (
        tokens, mix_gain.reshape(16, 128), w_bgate, w_cgate, w_value, in_scale, mix_taps, w_mixout,
        mixout_scale, ffn_gain.reshape(16, 128), w_upgate.T, w_upval.T, up_scale,
        jnp.swapaxes(ffn_taps, 0, 1), w_down, down_scale,
    )
    vmem = pltpu.VMEM

    def exchange_buffers(piece, kept):
        return (
            vmem((2, 4, 2, *piece), BF),
            vmem((2, 4, 2, *piece), BF),
            vmem((2, 4, kept, *piece), F32),
            vmem((2, 2, *piece), BF),
            vmem((2, 2, 2, *piece), BF),
            vmem((2, 2, *piece), BF),
            vmem((2, 2, 2, *piece), BF),
        )

    dma = pltpu.SemaphoreType.DMA
    return pl.pallas_call(
        kernel,
        out_shape=jax.ShapeDtypeStruct(tokens.shape, BF),
        in_specs=[pl.BlockSpec(memory_space=pl.ANY)] * len(args),
        out_specs=pl.BlockSpec(memory_space=pltpu.VMEM),
        scratch_shapes=[
            *(vmem(a.shape, a.dtype) for a in args[1:]),
            vmem((3, 4, 4, 128, W), BF),
            vmem((1, 4, 4, 256, 128), BF),
            vmem((5, 4, 4, 128, W), BF),
            vmem((1, 4, 4, 128, 128), BF),
            vmem((1, 4, 4, 64, 128), BF),
            vmem((2, 4, 4, 64, 640), BF),
            vmem((2, SEQ, D), BF),
            vmem((2, SEQ, D), BF),
            vmem((2, SEQ, W), F32),
            vmem((2, SEQ, W), BF),
            vmem((2, SEQ, 896), BF),
            vmem((2, SEQ, 128), F32),
            vmem((2, SEQ, 128), F32),
            vmem((2, 5, SEQ, W), F32),
            vmem((2, SEQ, 128), F32),
            *exchange_buffers((HALF, W), 2),
            *exchange_buffers((64, 2 * SEQ), 4),
            dma((ROUNDS, 2, 8)),
            dma((ROUNDS, 2, 8)),
            dma((4, 8)),
            dma((4, 8)),
            dma((4, 10)),
            dma((4, 10)),
            dma((17,)),
        ],
        compiler_params=pltpu.CompilerParams(
            collective_id=0, has_side_effects=True, vmem_limit_bytes=62 * 1024 * 1024
        ),
        name="layer",
    )(*args)


def solution(mesh):
    return jax.shard_map(
        on_device,
        mesh=mesh,
        in_specs=(
            P("fs", None, "tp"),
            P(),
            P("fs", "tp"),
            P("fs", "tp"),
            P("fs", "tp"),
            P(None, "tp"),
            P(None, "tp"),
            P("tp", "fs"),
            P(None, "fs"),
            P(),
            P("fs", "tp"),
            P("fs", "tp"),
            P(None, "tp"),
            P(None, None, "tp"),
            P("tp", "fs"),
            P(None, "fs"),
        ),
        out_specs=P("fs", None, "tp"),
        check_vma=False,
    )
```

time: 112 us -> 113 us (level)
  no operation moved by 1% of the time
where the time goes in v3:
time: 113 us
  Pallas kernels  111 us (98%)
  local copies, waits for them, and re-layouts  1.77 us (2%)
    pallas_call x1, Pallas kernels, on_device(): pl.pallas_call(kernel, out_shape=jax.ShapeDtypeStruct(tokens.shape, BF),...  111 us

profile of v3, /device:TPU:1, one launch (start us, length us, event | category | flops | bytes accessed | tf_op | source)
XLA Modules:
  0.0 112.6 jit_solution(11626236597693439587)
XLA Ops:
  0.0 110.8 %layer.1 = bf16[2,384,256]{2,1,0:T(8,128)(2,1)} custom-call(bf16[2,384,256]{2,1,0:T(8,128)(2,1)} %tok_h.1, f32[16,128]{1,0:T(8,128)} %bitcast.8, f32[128,256]{1,0:T(8,128)} %wb_h.1, f32[128,256]{1,0:T(8,128)} %wc_h.1, f32[128,256]{1,0:T(8,128)} %wv_h.1, f32[3,256]{1,0:T(4,128)} %insc_h.1, f32[3,256]{1,0:T(4,128)} %mtaps_h.1, f32[256,128]{1,0:T(8,128)} %wm_h.1, ...), custom_call_target="tpu_custom_call" | custom-call | tf_op jit(solution)/shard_map/layer/pallas_call | solution.py:548
  110.8 1.8 %copy.18 = bf16[2,384,256]{2,1,0:T(8,128)(2,1)} copy(bf16[2,384,256]{2,1,0:T(8,128)(2,1)} %layer.1) | data formatting | bytes 786432

commit v4 on v3

--- a/solution.py
+++ b/solution.py
@@ -43,6 +43,10 @@
     pos = (y, z)
     sent = []
 
+    def slot(zz):
+        return (zz - x + 5) % 4
+
+
     def push(src, dst, ssem, rsem, dev):
         pltpu.make_async_remote_copy(
             src_ref=src, dst_ref=dst, send_sem=ssem, recv_sem=rsem,
@@ -66,11 +70,11 @@
         loads[name] = pltpu.make_async_copy(src, dst, load_sem.at[len(loads)])
         loads[name].start()
 
-    def cols_of(xx, cc):
-        return pl.ds(pl.multiple_of((xx * 2 + cc) * W, W), W)
+    def cols_of(place, cc):
+        return pl.ds(pl.multiple_of((place * 2 + cc) * W, W), W)
 
     for s in range(2):
-        load(("tok", s), tok_h.at[s], tfull.at[s, :, cols_of(x, core)])
+        load(("tok", s), tok_h.at[s], tfull.at[s, :, cols_of(1, core)])
     for name, src, dst in (
         ("mgain", mgain_h, mgain), ("insc", insc_h, insc), ("wc", wc_h, wc), ("wv", wv_h, wv), ("wb", wb_h, wb),
         ("msc", msc_h, msc), ("wm", wm_h, wm), ("fgain", fgain_h, fgain), ("upsc", upsc_h, upsc),
@@ -89,42 +93,44 @@
 
     tail = slice(640, 704)
 
+    mine = slot(z)
+
     def pack(r):
         if r < 3:
             w, row = ((wc, 1), (wv, 2), (wb, 0))[r]
             ready("mgain", "insc", ("wc", "wv", "wb")[r])
             col = jnp.broadcast_to(mgain[pl.ds(fs, 1), :], (128, 128)).T
             col = jnp.concatenate([col, col], axis=1)
-            g_in[r, z, y] = (rounded(w[...]) * col * insc[row : row + 1, :]).astype(BF)
+            g_in[r, mine, y] = (rounded(w[...]) * col * insc[row : row + 1, :]).astype(BF)
         elif r == 3:
             ready("msc", "wm")
-            g_mo[0, z, y] = (rounded(wm[...]) * msc[...]).astype(BF)
+            g_mo[0, mine, y] = (rounded(wm[...]) * msc[...]).astype(BF)
         elif r < 9:
             ready("fgain", "upsc", "wug", "wuv")
             frow = fgain[pl.ds(fs, 1), :]
             j = r - 4
             cols = slice(128 * j, 128 * j + 128)
             for k, w in enumerate((wug, wuv)):
-                g_up[j, z, y, :, 128 * k : 128 * k + 128] = (
+                g_up[j, mine, y, :, 128 * k : 128 * k + 128] = (
                     (rounded(w[cols, :]) * frow).T * upsc[k : k + 1, cols]
                 ).astype(BF)
         elif r == 9:
             frow = fgain[pl.ds(fs, 1), :]
             both = rounded(jnp.concatenate([wug[tail, :], wuv[tail, :]], axis=0))
             tail_scale = jnp.concatenate([upsc[0:1, tail], upsc[1:2, tail]], axis=1)
-            g_ul[0, z, y] = ((both * frow).T * tail_scale).astype(BF)
+            g_ul[0, mine, y] = ((both * frow).T * tail_scale).astype(BF)
         elif r == 10:
             ready("dsc", "wd")
             last = rounded(wd[tail, :]) * dsc[...]
             turned = jnp.concatenate([last, last], axis=0).T
             lane = lax.broadcasted_iota(jnp.int32, (64, 128), 1)
-            g_dt[0, z, y] = jnp.where(lane < 64, turned[0:64], turned[64:128]).astype(BF)
+            g_dt[0, mine, y] = jnp.where(lane < 64, turned[0:64], turned[64:128]).astype(BF)
         elif r < 13:
             lo = 64 * (r - 11)
             for j in range(5):
                 cols = slice(128 * j, 128 * j + 128)
                 turned = (rounded(wd[cols, :]) * dsc[...]).T
-                g_d[r - 11, z, y, :, cols] = turned[lo : lo + 64].astype(BF)
+                g_d[r - 11, mine, y, :, cols] = turned[lo : lo + 64].astype(BF)
 
     rounds = (
         [(g_in, k, 128) for k in range(3)]
@@ -137,12 +143,12 @@
     def block(r, h, p_at, q_at, lo, n):
         ref, k, rows = rounds[r]
         zz, yy = (q_at, p_at) if h == 0 else (p_at, q_at)
-        return ref.at[k, zz, yy, pl.ds(lo, n), :]
+        return ref.at[k, slot(zz), yy, pl.ds(lo, n), :]
 
     def line(r, h, q_at, lo, n):
         ref, k, rows = rounds[r]
         if h == 0:
-            return ref.at[k, q_at, pl.ds(0, 4), pl.ds(lo, n), :]
+            return ref.at[k, slot(q_at), pl.ds(0, 4), pl.ds(lo, n), :]
         return ref.at[k, pl.ds(0, 4), q_at, pl.ds(lo, n), :]
 
     def geometry(r, h):
@@ -216,46 +222,51 @@
         ahead(k)
         s4(k - 1)
 
-    def gather_own(u, buf, s, src):
-        dst = buf.at[s, :, cols_of(x, core)]
-        send(src, dst, a_send.at[u, 0], a_recv.at[u, 0], dev_xp)
-        send(src, dst, a_send.at[u, 1], a_recv.at[u, 1], dev_xm)
-        send(src, dst, a_send.at[u, 2], a_recv.at[u, 4], dev_sib)
+    def gather_own(u, buf, s):
+        src = buf.at[s, :, cols_of(1, core)]
+        send(src, buf.at[s, :, cols_of(0, core)], a_send.at[u, 0], a_recv.at[u, 0], dev_xp)
+        send(src, buf.at[s, :, cols_of(2, core)], a_send.at[u, 1], a_recv.at[u, 1], dev_xm)
+        send(src, src, a_send.at[u, 2], a_recv.at[u, 4], dev_sib)
 
     def gather_near(u, buf, s):
-        for d, xx, lo, dev in ((0, xm, 0, dev_xp), (1, xp, HALF, dev_xm)):
-            whole = buf.at[s, :, cols_of(xx, core)]
+        for d, place, lo, dev in ((0, 0, 0, dev_xp), (1, 2, HALF, dev_xm)):
+            whole = buf.at[s, :, cols_of(place, core)]
             arrived(whole, a_recv.at[u, d])
-            piece = buf.at[s, pl.ds(lo, HALF), cols_of(xx, core)]
-            send(piece, piece, a_send.at[u, 3 + d], a_recv.at[u, 2 + d], dev)
+            rows = pl.ds(lo, HALF)
+            send(
+                buf.at[s, rows, cols_of(place, core)], buf.at[s, rows, cols_of(3, core)],
+                a_send.at[u, 3 + d], a_recv.at[u, 2 + d], dev,
+            )
             send(whole, whole, a_send.at[u, 5 + d], a_recv.at[u, 5 + d], dev_sib)
 
     def gather_far(u, buf, s):
         for d, lo in ((0, 0), (1, HALF)):
-            arrived(buf.at[s, pl.ds(lo, HALF), cols_of(xf, core)], a_recv.at[u, 2 + d])
-        whole = buf.at[s, :, cols_of(xf, core)]
+            arrived(buf.at[s, pl.ds(lo, HALF), cols_of(3, core)], a_recv.at[u, 2 + d])
+        whole = buf.at[s, :, cols_of(3, core)]
         send(whole, whole, a_send.at[u, 7], a_recv.at[u, 7], dev_sib)
 
-    def gather_done(u, buf, s):
-        for k, xx in ((4, x), (5, xm), (6, xp), (7, xf)):
-            arrived(buf.at[s, :, cols_of(xx, 1 - core)], a_recv.at[u, k])
-
-    def wide_cols(xx):
-        return pl.ds(pl.multiple_of(xx * 2 * W, 2 * W), 2 * W)
-
-    def add_squares(buf, s, xx, first=False):
-        v = buf[s, :, wide_cols(xx)].astype(F32)
-        v = v * v
-        total = v[:, 0:128] + v[:, 128:256] + v[:, 256:384] + v[:, 384:512]
-        squares[s] = total if first else squares[s] + total
+    def near_done(u, buf, s):
+        for k, place in ((4, 1), (5, 0), (6, 2)):
+            arrived(buf.at[s, :, cols_of(place, 1 - core)], a_recv.at[u, k])
+
+    def far_done(u, buf, s):
+        arrived(buf.at[s, :, cols_of(3, 1 - core)], a_recv.at[u, 7])
+
+    def add_squares(buf, s, places):
+        total = None
+        for j in range(4 * places[0], 4 * places[1]):
+            v = buf[s, :, 128 * j : 128 * j + 128].astype(F32)
+            total = v * v if total is None else total + v * v
+        squares[s] = total if places[0] == 0 else squares[s] + total
 
     def row_factor(s):
         mean = jnp.sum(squares[s], axis=1, keepdims=True) * (1.0 / D)
         fac[s] = jnp.broadcast_to(lax.rsqrt(mean + EPS), (SEQ, 128))
 
     def shifted(v, n):
-        row = lax.broadcasted_iota(jnp.int32, v.shape, 0)
-        return jnp.where(row >= n, pltpu.roll(v, n, 0), 0.0)
+        turned = pltpu.roll(v, n, 0)
+        row = lax.broadcasted_iota(jnp.int32, (8, v.shape[1]), 0)
+        return jnp.concatenate([jnp.where(row >= n, turned[0:8], 0.0), turned[8:]], axis=0)
 
     def causal(v, taps):
         return shifted(v, 2) * taps[0:1] + shifted(v, 1) * taps[1:2] + v * taps[2:3]
@@ -264,7 +275,7 @@
         f = fac[s]
         return jnp.concatenate([f, f], axis=1)
 
-    order = (xf, xp, xm, x)
+    order = (3, 2, 0, 1)
 
     class Unit:
         def __init__(self, u, sems, sb, rb, keep, fbuf, nbuf, rf, rn):
@@ -317,7 +328,7 @@
 
     def ffn_unit(h):
         return Unit(
-            h, 2 + h, sb2, rb2, lambda k, d: keep2[h, k, 2 * core + d], fbuf2, nbuf2, rf2, rn2
+            h, 2 + h, sb2, rb2, lambda k, d: keep2[h, order[k], 2 * core + d], fbuf2, nbuf2, rf2, rn2
         )
 
     def dot(a, b):
@@ -341,71 +352,64 @@
             gated[s] = (dot(tfull[s], g_in[2].reshape(D, W)) * cbuf[s]).astype(BF)
 
     def mix_parts(s, unit):
-        for k, xx in enumerate(order):
-            for cc in (1 - core, core):
-                mat = jnp.concatenate([g_mo[0, xx, 2 * cc], g_mo[0, xx, 2 * cc + 1]], axis=1)
-                term = dot(gated[s], mat).reshape(2, HALF, W)
+        for cc in (1 - core, core):
+            mat = jnp.concatenate([g_mo[0, place, 2 * cc + j] for place in order for j in range(2)], axis=1)
+            term = dot(gated[s], mat)
+            for k in range(4):
+                piece = term[:, W * k : W * k + W].reshape(2, HALF, W)
                 if cc is core:
-                    keep[s, k] = term
+                    keep[s, k] = piece
                 else:
-                    sb[s, k] = term.astype(BF)
+                    sb[s, k] = piece.astype(BF)
                     unit.part(k)
 
-    def up_dots(s, j, blocks):
-        total = None
-        for xx in blocks:
-            mat = g_ul[0, xx].reshape(512, 128) if j is None else g_up[j, xx].reshape(512, W)
-            term = dot(rfull[s, :, wide_cols(xx)], mat)
-            total = term if total is None else total + term
-        return total
-
-    def up_first(s):
-        @pl.loop(0, 5)
-        def _(j):
-            acc[s, j] = up_dots(s, j, (x, xm, xp))
-
-        acc_tail[s] = up_dots(s, None, (x, xm, xp))
+    def up_first(s, js):
+        for j in js:
+            if j < 5:
+                acc[s, j] = dot(rfull[s, :, 0:1536], g_up[j, 0:3].reshape(1536, W))
+            else:
+                acc_tail[s] = dot(rfull[s, :, 0:1536], g_ul[0, 0:3].reshape(1536, 128))
+
+    def tokens_of(s):
+        return slice(SEQ * s, SEQ * s + SEQ)
 
     def silu(v):
         return v / (1.0 + jnp.exp(-v))
 
     def up_second(s):
-        @pl.loop(0, 5)
-        def _(j):
-            cols = pl.ds(pl.multiple_of(128 * j, 128), 128)
-            pre = (acc[s, j] + up_dots(s, j, (xf,))) * wide(s)
+        for j in range(5):
+            cols = slice(128 * j, 128 * j + 128)
+            pre = (acc[s, j] + dot(rfull[s, :, 1536:2048], g_up[j, 3].reshape(512, W))) * wide(s)
             taps = jnp.concatenate([ftaps[:, 0, cols], ftaps[:, 1, cols]], axis=1)
             conv = causal(pre, taps)
-            active[s, :, cols] = (silu(conv[:, 0:128]) * conv[:, 128:256]).astype(BF)
-
-        pre = (acc_tail[s] + up_dots(s, None, (xf,))) * fac[s]
+            active[cols, tokens_of(s)] = (silu(conv[:, 0:128]) * conv[:, 128:256]).T.astype(BF)
+        pre = (acc_tail[s] + dot(rfull[s, :, 1536:2048], g_ul[0, 3].reshape(512, 128))) * fac[s]
         taps = jnp.concatenate([ftaps[:, 0, tail], ftaps[:, 1, tail]], axis=1)
         conv = causal(pre, taps)
-        act = silu(conv) * pltpu.roll(conv, 64, 1)
-        lane = lax.broadcasted_iota(jnp.int32, (SEQ, 128), 1)
-        act = jnp.where(lane < 64, act, 0.0)
-        active[s, :, 640:768] = act.astype(BF)
-        active[s, :, 768:896] = pltpu.roll(act, 64, 1).astype(BF)
-
-    def turned_dot(a, b):
-        return lax.dot_general(a, b, (((1,), (1,)), ((), ())), preferred_element_type=F32)
+        act = (silu(conv) * pltpu.roll(conv, 64, 1)).T[0:64].astype(BF)
+        active[640:704, tokens_of(s)] = act
+        active[832:896, tokens_of(s)] = act
+        active[704:832, tokens_of(s)] = jnp.zeros((128, SEQ), BF)
 
     def down_parts(h, unit):
-        for k, xx in enumerate(order):
-            for s in range(2):
-                term = turned_dot(g_d[h, xx].reshape(256, 640), active[s, :, 0:640])
-                lo = 640 + 128 * h
-                term = term + turned_dot(g_dt[0, xx].reshape(256, 128), active[s, :, lo : lo + 128])
-                keep2[h, k, :, :, SEQ * s : SEQ * s + SEQ] = term.reshape(4, 64, SEQ)
-            sb2[h, k] = keep2[h, k, pl.ds(2 * (1 - core), 2)].astype(BF)
-            unit.part(k)
-
-    own = cols_of(x, core)
+        lo = 640 + 128 * h
+        acts = jnp.concatenate([active[0:640, :], active[lo : lo + 128, :]], axis=0)
+        for first, ks in ((2, (0, 1)), (0, (2, 3))):
+            places = slice(first, first + 2)
+            mat = jnp.concatenate(
+                [g_d[h, places].reshape(512, 640), g_dt[0, places].reshape(512, 128)], axis=1
+            )
+            keep2[h, places] = dot(mat, acts).reshape(2, 4, 64, 2 * SEQ)
+            for k in ks:
+                sb2[h, k] = keep2[h, order[k], pl.ds(2 * (1 - core), 2)].astype(BF)
+                unit.part(k)
+
+    own = cols_of(1, core)
 
     ready(("tok", 0), ("tok", 1))
     pl.semaphore_wait(barrier, 7)
     for s in range(2):
-        gather_own(s, tfull, s, tfull.at[s, :, own])
+        gather_own(s, tfull, s)
     pack(0)
     s1(0)
     s1(1)
@@ -415,15 +419,18 @@
     tick(1)
     gather_near(1, tfull, 1)
     gather_far(0, tfull, 0)
+    near_done(0, tfull, 0)
+    add_squares(tfull, 0, (0, 3))
     tick(2)
     gather_far(1, tfull, 1)
     ready("mtaps", "ftaps")
+    ahead(3)
+    near_done(1, tfull, 1)
+    add_squares(tfull, 1, (0, 3))
     for s in range(2):
-        gather_done(s, tfull, s)
-        for xx in range(4):
-            add_squares(tfull, s, xx, xx == 0)
+        far_done(s, tfull, s)
+        add_squares(tfull, s, (3, 4))
         row_factor(s)
-    ahead(3)
     done(0)
     in_cgate()
     s4(2)
@@ -437,63 +444,68 @@
     done(3)
     u0, u1 = mix_unit(0), mix_unit(1)
     mix_parts(0, u0)
+    s4(4)
+    s1(8)
+    s2(7)
     u0.far()
     u0.near()
-    s4(4)
+    s3(6)
     mix_parts(1, u1)
+    s4(5)
     u1.far()
-    ahead(6)
     u0.last()
     u1.near()
-    s4(5)
+    s1(9)
+    s2(8)
+    s3(7)
+    s4(6)
+    s1(10)
     u1.last()
-    ahead(7)
+    s2(9)
+    s1(11)
+    s3(8)
 
     def residual(s, unit):
         unit.landed()
         for d in range(2):
             rows = slice(HALF * d, HALF * d + HALF)
             rfull[s, rows, own] = (tfull[s, rows, own].astype(F32) + unit.total(d)).astype(BF)
-        gather_own(2 + s, rfull, s, rfull.at[s, :, own])
+        gather_own(2 + s, rfull, s)
 
     residual(0, u0)
-    s4(6)
-    ahead(8)
+    s4(7)
+    s2(10)
     residual(1, u1)
+    s1(12)
+    s3(9)
+    s2(11)
     gather_near(2, rfull, 0)
-    s4(7)
-    ahead(9)
+    s4(8)
+    s3(10)
+    near_done(2, rfull, 0)
+    add_squares(rfull, 0, (0, 3))
     for r in range(4, 8):
         done(r)
+    s4(9)
+    up_first(0, (0, 1, 2, 3))
     gather_near(3, rfull, 1)
-    tick(10)
-
-    def near_done(u, buf, s):
-        for k, xx in ((4, x), (5, xm), (6, xp)):
-            arrived(buf.at[s, :, cols_of(xx, 1 - core)], a_recv.at[u, k])
-
-    def far_done(u, buf, s):
-        arrived(buf.at[s, :, cols_of(xf, 1 - core)], a_recv.at[u, 7])
-
-    s4(8)
-    tick(11)
+    s2(12)
+    s3(11)
+    s4(10)
     done(8)
     done(9)
-    near_done(2, rfull, 0)
-    for k, xx in enumerate((x, xm, xp)):
-        add_squares(rfull, 0, xx, k == 0)
-    up_first(0)
+    up_first(0, (4, 5))
+    near_done(3, rfull, 1)
     gather_far(2, rfull, 0)
-    tick(12)
-    near_done(3, rfull, 1)
-    for k, xx in enumerate((x, xm, xp)):
-        add_squares(rfull, 1, xx, k == 0)
-    up_first(1)
+    s3(12)
+    s4(11)
+    add_squares(rfull, 1, (0, 3))
+    up_first(1, (0, 1, 2, 3, 4, 5))
     gather_far(3, rfull, 1)
-    tick(13)
+    s4(12)
     for s in range(2):
         far_done(2 + s, rfull, s)
-        add_squares(rfull, s, xf)
+        add_squares(rfull, s, (3, 4))
         row_factor(s)
         up_second(s)
     done(10)
@@ -516,7 +528,7 @@
         for d in range(2):
             lanes = slice(SEQ * s, SEQ * s + SEQ)
             turned = jnp.concatenate([total[0][d][:, lanes], total[1][d][:, lanes]], axis=0).T
-            cols = pl.ds(pl.multiple_of((x * 2 + core) * W + 128 * d, 128), 128)
+            cols = pl.ds(pl.multiple_of((2 + core) * W + 128 * d, 128), 128)
             out[s, :, 128 * d : 128 * d + 128] = (rfull[s, :, cols].astype(F32) + turned).astype(BF)
     for src, ssem in sent:
         arrived(src, ssem)
@@ -562,7 +574,7 @@
             vmem((2, SEQ, D), BF),
             vmem((2, SEQ, W), F32),
             vmem((2, SEQ, W), BF),
-            vmem((2, SEQ, 896), BF),
+            vmem((896, 2 * SEQ), BF),
             vmem((2, SEQ, 128), F32),
             vmem((2, SEQ, 128), F32),
             vmem((2, 5, SEQ, W), F32),

time: 113 us -> 105 us (0.929)
  Pallas kernels: 111 us -> 103 us
    pallas_call x1, Pallas kernels: 111 us -> 103 us  [on_device(): pl.pallas_call(kernel, out_shape=jax.ShapeDtypeStruct(tokens.shape, BF),...]
where the time goes in v4:
time: 105 us
  Pallas kernels  103 us (98%)
  local copies, waits for them, and re-layouts  1.77 us (2%)
    pallas_call x1, Pallas kernels, on_device(): pl.pallas_call(kernel, out_shape=jax.ShapeDtypeStruct(tokens.shape, BF),...  103 us

profile of v4, /device:TPU:1, one launch (start us, length us, event | category | flops | bytes accessed | tf_op | source)
XLA Modules:
  0.0 104.6 jit_solution(8051973557653490411)
XLA Ops:
  0.0 102.8 %layer.1 = bf16[2,384,256]{2,1,0:T(8,128)(2,1)} custom-call(bf16[2,384,256]{2,1,0:T(8,128)(2,1)} %tok_h.1, f32[16,128]{1,0:T(8,128)} %bitcast.8, f32[128,256]{1,0:T(8,128)} %wb_h.1, f32[128,256]{1,0:T(8,128)} %wc_h.1, f32[128,256]{1,0:T(8,128)} %wv_h.1, f32[3,256]{1,0:T(4,128)} %insc_h.1, f32[3,256]{1,0:T(4,128)} %mtaps_h.1, f32[256,128]{1,0:T(8,128)} %wm_h.1, ...), custom_call_target="tpu_custom_call" | custom-call | tf_op jit(solution)/shard_map/layer/pallas_call | solution.py:560
  102.8 1.8 %copy.18 = bf16[2,384,256]{2,1,0:T(8,128)(2,1)} copy(bf16[2,384,256]{2,1,0:T(8,128)(2,1)} %layer.1) | data formatting | bytes 786432

commit v5 on v4

--- a/solution.py
+++ b/solution.py
@@ -53,10 +53,6 @@
             device_id=dev, device_id_type=pl.DeviceIdType.MESH,
         ).start()
 
-    def send(src, dst, ssem, rsem, dev):
-        push(src, dst, ssem, rsem, dev)
-        sent.append((src, ssem))
-
     def arrived(dst, rsem):
         pltpu.make_async_copy(dst, dst, rsem).wait()
 
@@ -73,10 +69,9 @@
     def cols_of(place, cc):
         return pl.ds(pl.multiple_of((place * 2 + cc) * W, W), W)
 
-    for s in range(2):
-        load(("tok", s), tok_h.at[s], tfull.at[s, :, cols_of(1, core)])
+    load("tok", tok_h, tfull.at[:, :, cols_of(1, core)])
     for name, src, dst in (
-        ("mgain", mgain_h, mgain), ("insc", insc_h, insc), ("wc", wc_h, wc), ("wv", wv_h, wv), ("wb", wb_h, wb),
+        ("wc", wc_h, wc), ("mgain", mgain_h, mgain), ("insc", insc_h, insc), ("wv", wv_h, wv), ("wb", wb_h, wb),
         ("msc", msc_h, msc), ("wm", wm_h, wm), ("fgain", fgain_h, fgain), ("upsc", upsc_h, upsc),
         ("wug", wug_h, wug), ("wuv", wuv_h, wuv), ("dsc", dsc_h, dsc), ("wd", wd_h, wd),
         ("mtaps", mtaps_h, mtaps), ("ftaps", ftaps_h, ftaps),
@@ -93,7 +88,7 @@
 
     tail = slice(640, 704)
 
-    mine = slot(z)
+    mine = slot(z) * 4 + y
 
     def pack(r):
         if r < 3:
@@ -101,36 +96,36 @@
             ready("mgain", "insc", ("wc", "wv", "wb")[r])
             col = jnp.broadcast_to(mgain[pl.ds(fs, 1), :], (128, 128)).T
             col = jnp.concatenate([col, col], axis=1)
-            g_in[r, mine, y] = (rounded(w[...]) * col * insc[row : row + 1, :]).astype(BF)
+            g_in[r, mine] = (rounded(w[...]) * col * insc[row : row + 1, :]).astype(BF)
         elif r == 3:
             ready("msc", "wm")
-            g_mo[0, mine, y] = (rounded(wm[...]) * msc[...]).astype(BF)
+            g_mo[0, mine] = (rounded(wm[...]) * msc[...]).astype(BF)
         elif r < 9:
             ready("fgain", "upsc", "wug", "wuv")
             frow = fgain[pl.ds(fs, 1), :]
             j = r - 4
             cols = slice(128 * j, 128 * j + 128)
             for k, w in enumerate((wug, wuv)):
-                g_up[j, mine, y, :, 128 * k : 128 * k + 128] = (
+                g_up[j, mine, :, 128 * k : 128 * k + 128] = (
                     (rounded(w[cols, :]) * frow).T * upsc[k : k + 1, cols]
                 ).astype(BF)
         elif r == 9:
             frow = fgain[pl.ds(fs, 1), :]
             both = rounded(jnp.concatenate([wug[tail, :], wuv[tail, :]], axis=0))
             tail_scale = jnp.concatenate([upsc[0:1, tail], upsc[1:2, tail]], axis=1)
-            g_ul[0, mine, y] = ((both * frow).T * tail_scale).astype(BF)
+            g_ul[0, mine] = ((both * frow).T * tail_scale).astype(BF)
         elif r == 10:
             ready("dsc", "wd")
             last = rounded(wd[tail, :]) * dsc[...]
             turned = jnp.concatenate([last, last], axis=0).T
             lane = lax.broadcasted_iota(jnp.int32, (64, 128), 1)
-            g_dt[0, mine, y] = jnp.where(lane < 64, turned[0:64], turned[64:128]).astype(BF)
+            g_dt[0, mine] = jnp.where(lane < 64, turned[0:64], turned[64:128]).astype(BF)
         elif r < 13:
             lo = 64 * (r - 11)
             for j in range(5):
                 cols = slice(128 * j, 128 * j + 128)
                 turned = (rounded(wd[cols, :]) * dsc[...]).T
-                g_d[r - 11, mine, y, :, cols] = turned[lo : lo + 64].astype(BF)
+                g_d[r - 11, mine, :, cols] = turned[lo : lo + 64].astype(BF)
 
     rounds = (
         [(g_in, k, 128) for k in range(3)]
@@ -143,18 +138,24 @@
     def block(r, h, p_at, q_at, lo, n):
         ref, k, rows = rounds[r]
         zz, yy = (q_at, p_at) if h == 0 else (p_at, q_at)
-        return ref.at[k, slot(zz), yy, pl.ds(lo, n), :]
-
-    def line(r, h, q_at, lo, n):
-        ref, k, rows = rounds[r]
-        if h == 0:
-            return ref.at[k, slot(q_at), pl.ds(0, 4), pl.ds(lo, n), :]
-        return ref.at[k, pl.ds(0, 4), q_at, pl.ds(lo, n), :]
+        return ref.at[k, slot(zz) * 4 + yy, pl.ds(lo, n), :]
+
+    def some(r, n, rows):
+        ref, k, _ = rounds[r]
+        return ref.at[k, pl.ds(0, n), pl.ds(0, rows), :]
 
     def geometry(r, h):
         half = rounds[r][2] // 2
         lo = half * h
         return lo, half, lo, lo + half // 2, half // 2, pos[h], pos[1 - h]
+
+    def hop(r, h, stage, piece, axis, d):
+        push(piece, piece, y_send.at[r], y_recv.at[r, 2 * stage + h if stage < 3 else 6], dev_axis[axis][d])
+
+    def across(r, h, p_at):
+        lo, half, up, dn, quarter, p, q = geometry(r, h)
+        for d in range(2):
+            hop(r, h, 2, block(r, h, p_at, q, lo, half), 1 - h, d)
 
     def s1(r):
         if not 0 <= r < ROUNDS:
@@ -162,26 +163,19 @@
         pack(r + 1)
         for h in range(2):
             lo, half, up, dn, quarter, p, q = geometry(r, h)
-            own = block(r, h, p, q, lo, half)
             for d in range(2):
-                send(own, own, y_send.at[r, h, d], y_recv.at[r, h, d], dev_axis[h][d])
+                hop(r, h, 0, block(r, h, p, q, lo, half), h, d)
             across(r, h, p)
-
-    def across(r, h, p_at):
-        lo, half, up, dn, quarter, p, q = geometry(r, h)
-        piece = block(r, h, p_at, q, lo, half)
-        for d in range(2):
-            push(piece, piece, y_send.at[r, h, 4 + d], y_recv.at[r, h, 4 + d], dev_axis[1 - h][d])
 
     def s2(r):
         if not 0 <= r < ROUNDS:
             return
         for h in range(2):
             lo, half, up, dn, quarter, p, q = geometry(r, h)
+            arrived(some(r, 2, half), y_recv.at[r, h])
             for d, at, part in ((0, (p + 3) % 4, up), (1, (p + 1) % 4, dn)):
-                arrived(block(r, h, at, q, lo, half), y_recv.at[r, h, d])
-                piece = block(r, h, at, q, part, quarter)
-                send(piece, piece, y_send.at[r, h, 2 + d], y_recv.at[r, h, 2 + d], dev_axis[h][d])
+                hop(r, h, 1, block(r, h, at, q, part, quarter), h, d)
+            for at in ((p + 3) % 4, (p + 1) % 4):
                 across(r, h, at)
 
     def s3(r):
@@ -189,29 +183,22 @@
             return
         for h in range(2):
             lo, half, up, dn, quarter, p, q = geometry(r, h)
-            for d, part in ((0, up), (1, dn)):
-                arrived(block(r, h, (p + 2) % 4, q, part, quarter), y_recv.at[r, h, 2 + d])
+            arrived(some(r, 2, quarter), y_recv.at[r, 2 + h])
             across(r, h, (p + 2) % 4)
-            for d in range(2):
-                sent.append((line(r, h, q, lo, half), y_send.at[r, h, 4 + d]))
 
     def s4(r):
         if not 0 <= r < ROUNDS:
             return
         for h in range(2):
             lo, half, up, dn, quarter, p, q = geometry(r, h)
+            arrived(some(r, 8, half), y_recv.at[r, 4 + h])
             for d, at, part in ((0, (q + 3) % 4, up), (1, (q + 1) % 4, dn)):
-                arrived(line(r, h, at, lo, half), y_recv.at[r, h, 4 + d])
                 for k in range(4):
-                    piece = block(r, h, k, at, part, quarter)
-                    push(piece, piece, y_send.at[r, h, 6 + d], y_recv.at[r, h, 6 + d], dev_axis[1 - h][d])
-                sent.append((line(r, h, at, part, quarter), y_send.at[r, h, 6 + d]))
+                    hop(r, h, 3, block(r, h, k, at, part, quarter), 1 - h, d)
+        sent.append((some(r, 15, rounds[r][2]), y_send.at[r]))
 
     def done(r):
-        for h in range(2):
-            lo, half, up, dn, quarter, p, q = geometry(r, h)
-            for d, part in ((0, up), (1, dn)):
-                arrived(line(r, h, (q + 2) % 4, part, quarter), y_recv.at[r, h, 6 + d])
+        arrived(some(r, 16, rounds[r][2] // 4), y_recv.at[r, 6])
 
     def ahead(k):
         s1(k + 2)
@@ -224,33 +211,32 @@
 
     def gather_own(u, buf, s):
         src = buf.at[s, :, cols_of(1, core)]
-        send(src, buf.at[s, :, cols_of(0, core)], a_send.at[u, 0], a_recv.at[u, 0], dev_xp)
-        send(src, buf.at[s, :, cols_of(2, core)], a_send.at[u, 1], a_recv.at[u, 1], dev_xm)
-        send(src, src, a_send.at[u, 2], a_recv.at[u, 4], dev_sib)
+        push(src, buf.at[s, :, cols_of(0, core)], a_send.at[u], a_recv.at[u, 0], dev_xp)
+        push(src, buf.at[s, :, cols_of(2, core)], a_send.at[u], a_recv.at[u, 1], dev_xm)
+        push(src, src, a_send.at[u], a_recv.at[u, 3], dev_sib)
 
     def gather_near(u, buf, s):
         for d, place, lo, dev in ((0, 0, 0, dev_xp), (1, 2, HALF, dev_xm)):
             whole = buf.at[s, :, cols_of(place, core)]
             arrived(whole, a_recv.at[u, d])
             rows = pl.ds(lo, HALF)
-            send(
+            push(
                 buf.at[s, rows, cols_of(place, core)], buf.at[s, rows, cols_of(3, core)],
-                a_send.at[u, 3 + d], a_recv.at[u, 2 + d], dev,
+                a_send.at[u], a_recv.at[u, 2], dev,
             )
-            send(whole, whole, a_send.at[u, 5 + d], a_recv.at[u, 5 + d], dev_sib)
+            push(whole, whole, a_send.at[u], a_recv.at[u, 3], dev_sib)
 
     def gather_far(u, buf, s):
-        for d, lo in ((0, 0), (1, HALF)):
-            arrived(buf.at[s, pl.ds(lo, HALF), cols_of(3, core)], a_recv.at[u, 2 + d])
         whole = buf.at[s, :, cols_of(3, core)]
-        send(whole, whole, a_send.at[u, 7], a_recv.at[u, 7], dev_sib)
+        arrived(whole, a_recv.at[u, 2])
+        push(whole, whole, a_send.at[u], a_recv.at[u, 4], dev_sib)
+        sent.append((sb.at[pl.ds(0, 14)], a_send.at[u]))
 
     def near_done(u, buf, s):
-        for k, place in ((4, 1), (5, 0), (6, 2)):
-            arrived(buf.at[s, :, cols_of(place, 1 - core)], a_recv.at[u, k])
+        arrived(buf.at[s, :, pl.ds(0, 3 * W)], a_recv.at[u, 3])
 
     def far_done(u, buf, s):
-        arrived(buf.at[s, :, cols_of(3, 1 - core)], a_recv.at[u, 7])
+        arrived(buf.at[s, :, cols_of(3, 1 - core)], a_recv.at[u, 4])
 
     def add_squares(buf, s, places):
         total = None
@@ -279,46 +265,47 @@
 
     class Unit:
         def __init__(self, u, sems, sb, rb, keep, fbuf, nbuf, rf, rn):
-            self.sb, self.rb, self.fbuf, self.nbuf, self.rf, self.rn = (
-                ref.at[u] for ref in (sb, rb, fbuf, nbuf, rf, rn)
-            )
+            self.fbuf, self.nbuf, self.rf, self.rn = (ref.at[u] for ref in (fbuf, nbuf, rf, rn))
+            self.sb, self.rb, self.base = sb, rb, 8 * u
             self.keep = keep
             self.ssem, self.rsem = r_send.at[sems], r_recv.at[sems]
 
+        def pieces(self, ref, k, n=1):
+            return ref.at[pl.ds(self.base + 2 * k, 2 * n)]
+
         def part(self, k):
-            send(self.sb.at[k], self.rb.at[k], self.ssem.at[k], self.rsem.at[k], dev_sib)
+            push(
+                self.pieces(self.sb, k), self.pieces(self.rb, k),
+                self.ssem, self.rsem.at[(0, 1, 1, 3)[k]], dev_sib,
+            )
 
         def both(self, k, d):
-            return self.keep(k, d) + self.rb[k, d].astype(F32)
+            return self.keep(k, d) + self.rb[self.base + 2 * k + d].astype(F32)
 
         def far(self):
-            arrived(self.rb.at[0], self.rsem.at[0])
-            for d, dev in ((0, dev_xp), (1, dev_xm)):
+            arrived(self.pieces(self.rb, 0), self.rsem.at[0])
+            for d in range(2):
                 self.fbuf[d] = self.both(0, d).astype(BF)
             for d, dev in ((0, dev_xp), (1, dev_xm)):
-                send(self.fbuf.at[d], self.rf.at[d], self.ssem.at[4 + d], self.rsem.at[4 + d], dev)
+                push(self.fbuf.at[d], self.rf.at[d], self.ssem, self.rsem.at[2], dev)
 
         def near(self):
-            for d, dev in ((0, dev_xp), (1, dev_xm)):
-                arrived(self.rb.at[1 + d], self.rsem.at[1 + d])
+            arrived(self.pieces(self.rb, 1, 2), self.rsem.at[1])
+            for d in range(2):
                 self.nbuf[d, 1 - d] = self.both(1 + d, 1 - d).astype(BF)
             for d, dev in ((0, dev_xp), (1, dev_xm)):
-                send(
-                    self.nbuf.at[d, 1 - d], self.rn.at[d, 1 - d],
-                    self.ssem.at[6 + d], self.rsem.at[6 + d], dev,
-                )
+                push(self.nbuf.at[d, 1 - d], self.rn.at[d, 1 - d], self.ssem, self.rsem.at[3], dev)
 
         def last(self):
+            arrived(self.rf, self.rsem.at[2])
+            for d in range(2):
+                self.nbuf[d, d] = (self.both(1 + d, d) + self.rf[d].astype(F32)).astype(BF)
             for d, dev in ((0, dev_xp), (1, dev_xm)):
-                arrived(self.rf.at[d], self.rsem.at[4 + d])
-                self.nbuf[d, d] = (self.both(1 + d, d) + self.rf[d].astype(F32)).astype(BF)
-                send(self.nbuf.at[d, d], self.rn.at[d, d], self.ssem.at[8 + d], self.rsem.at[8 + d], dev)
+                push(self.nbuf.at[d, d], self.rn.at[d, d], self.ssem, self.rsem.at[3], dev)
+            sent.append((sb.at[pl.ds(0, 14)], self.ssem))
 
         def landed(self):
-            arrived(self.rb.at[3], self.rsem.at[3])
-            for d in range(2):
-                arrived(self.rn.at[d, 1 - d], self.rsem.at[6 + d])
-                arrived(self.rn.at[d, d], self.rsem.at[8 + d])
+            arrived(self.rb.at[pl.ds(0, 6)], self.rsem.at[3])
 
         def total(self, d):
             return self.both(3, d) + self.rn[0, d].astype(F32) + self.rn[1, d].astype(F32)
@@ -328,7 +315,7 @@
 
     def ffn_unit(h):
         return Unit(
-            h, 2 + h, sb2, rb2, lambda k, d: keep2[h, order[k], 2 * core + d], fbuf2, nbuf2, rf2, rn2
+            h, 2 + h, sb2, rb2, lambda k, d: keep2[h, 4 * order[k] + 2 * core + d], fbuf2, nbuf2, rf2, rn2
         )
 
     def dot(a, b):
@@ -353,22 +340,22 @@
 
     def mix_parts(s, unit):
         for cc in (1 - core, core):
-            mat = jnp.concatenate([g_mo[0, place, 2 * cc + j] for place in order for j in range(2)], axis=1)
+            mat = jnp.concatenate([g_mo[0, 4 * place + 2 * cc + j] for place in order for j in range(2)], axis=1)
             term = dot(gated[s], mat)
             for k in range(4):
                 piece = term[:, W * k : W * k + W].reshape(2, HALF, W)
                 if cc is core:
                     keep[s, k] = piece
                 else:
-                    sb[s, k] = piece.astype(BF)
+                    sb[8 * s + 2 * k : 8 * s + 2 * k + 2] = piece.astype(BF)
                     unit.part(k)
 
     def up_first(s, js):
         for j in js:
             if j < 5:
-                acc[s, j] = dot(rfull[s, :, 0:1536], g_up[j, 0:3].reshape(1536, W))
+                acc[s, j] = dot(rfull[s, :, 0:1536], g_up[j, 0:12].reshape(1536, W))
             else:
-                acc_tail[s] = dot(rfull[s, :, 0:1536], g_ul[0, 0:3].reshape(1536, 128))
+                acc_tail[s] = dot(rfull[s, :, 0:1536], g_ul[0, 0:12].reshape(1536, 128))
 
     def tokens_of(s):
         return slice(SEQ * s, SEQ * s + SEQ)
@@ -379,11 +366,11 @@
     def up_second(s):
         for j in range(5):
             cols = slice(128 * j, 128 * j + 128)
-            pre = (acc[s, j] + dot(rfull[s, :, 1536:2048], g_up[j, 3].reshape(512, W))) * wide(s)
+            pre = (acc[s, j] + dot(rfull[s, :, 1536:2048], g_up[j, 12:16].reshape(512, W))) * wide(s)
             taps = jnp.concatenate([ftaps[:, 0, cols], ftaps[:, 1, cols]], axis=1)
             conv = causal(pre, taps)
             active[cols, tokens_of(s)] = (silu(conv[:, 0:128]) * conv[:, 128:256]).T.astype(BF)
-        pre = (acc_tail[s] + dot(rfull[s, :, 1536:2048], g_ul[0, 3].reshape(512, 128))) * fac[s]
+        pre = (acc_tail[s] + dot(rfull[s, :, 1536:2048], g_ul[0, 12:16].reshape(512, 128))) * fac[s]
         taps = jnp.concatenate([ftaps[:, 0, tail], ftaps[:, 1, tail]], axis=1)
         conv = causal(pre, taps)
         act = (silu(conv) * pltpu.roll(conv, 64, 1)).T[0:64].astype(BF)
@@ -395,26 +382,29 @@
         lo = 640 + 128 * h
         acts = jnp.concatenate([active[0:640, :], active[lo : lo + 128, :]], axis=0)
         for first, ks in ((2, (0, 1)), (0, (2, 3))):
-            places = slice(first, first + 2)
+            places = slice(4 * first, 4 * first + 8)
             mat = jnp.concatenate(
                 [g_d[h, places].reshape(512, 640), g_dt[0, places].reshape(512, 128)], axis=1
             )
-            keep2[h, places] = dot(mat, acts).reshape(2, 4, 64, 2 * SEQ)
+            keep2[h, places] = dot(mat, acts).reshape(8, 64, 2 * SEQ)
             for k in ks:
-                sb2[h, k] = keep2[h, order[k], pl.ds(2 * (1 - core), 2)].astype(BF)
+                piece = keep2[h, pl.ds(4 * order[k] + 2 * (1 - core), 2)].astype(BF)
+                sb2[8 * h + 2 * k : 8 * h + 2 * k + 2] = piece
                 unit.part(k)
 
     own = cols_of(1, core)
 
-    ready(("tok", 0), ("tok", 1))
+    pack(0)
+    ready("tok")
     pl.semaphore_wait(barrier, 7)
+    s1(0)
     for s in range(2):
         gather_own(s, tfull, s)
-    pack(0)
-    s1(0)
     s1(1)
+    s1(2)
     s2(0)
-    tick(0)
+    s2(1)
+    s3(0)
     gather_near(0, tfull, 0)
     tick(1)
     gather_near(1, tfull, 1)
@@ -492,22 +482,26 @@
     s2(12)
     s3(11)
     s4(10)
+    gather_far(2, rfull, 0)
     done(8)
     done(9)
     up_first(0, (4, 5))
     near_done(3, rfull, 1)
-    gather_far(2, rfull, 0)
-    s3(12)
-    s4(11)
     add_squares(rfull, 1, (0, 3))
     up_first(1, (0, 1, 2, 3, 4, 5))
+    s3(12)
     gather_far(3, rfull, 1)
-    s4(12)
-    for s in range(2):
+
+    def finish(s):
         far_done(2 + s, rfull, s)
         add_squares(rfull, s, (3, 4))
         row_factor(s)
         up_second(s)
+
+    finish(0)
+    s4(11)
+    finish(1)
+    s4(12)
     done(10)
     done(11)
     v0, v1 = ffn_unit(0), ffn_unit(1)
@@ -520,6 +514,8 @@
     v0.last()
     v1.near()
     v1.last()
+    for src, ssem in sent:
+        arrived(src, ssem)
     total = []
     for h, unit in enumerate((v0, v1)):
         unit.landed()
@@ -530,8 +526,6 @@
             turned = jnp.concatenate([total[0][d][:, lanes], total[1][d][:, lanes]], axis=0).T
             cols = pl.ds(pl.multiple_of((2 + core) * W + 128 * d, 128), 128)
             out[s, :, 128 * d : 128 * d + 128] = (rfull[s, :, cols].astype(F32) + turned).astype(BF)
-    for src, ssem in sent:
-        arrived(src, ssem)
 
 
 def on_device(
@@ -547,9 +541,9 @@
 
     def exchange_buffers(piece, kept):
         return (
-            vmem((2, 4, 2, *piece), BF),
-            vmem((2, 4, 2, *piece), BF),
-            vmem((2, 4, kept, *piece), F32),
+            vmem((16, *piece), BF),
+            vmem((16, *piece), BF),
+            vmem((2, *kept, *piece), F32),
             vmem((2, 2, *piece), BF),
             vmem((2, 2, 2, *piece), BF),
             vmem((2, 2, *piece), BF),
@@ -564,12 +558,12 @@
         out_specs=pl.BlockSpec(memory_space=pltpu.VMEM),
         scratch_shapes=[
             *(vmem(a.shape, a.dtype) for a in args[1:]),
-            vmem((3, 4, 4, 128, W), BF),
-            vmem((1, 4, 4, 256, 128), BF),
-            vmem((5, 4, 4, 128, W), BF),
-            vmem((1, 4, 4, 128, 128), BF),
-            vmem((1, 4, 4, 64, 128), BF),
-            vmem((2, 4, 4, 64, 640), BF),
+            vmem((3, 16, 128, W), BF),
+            vmem((1, 16, 256, 128), BF),
+            vmem((5, 16, 128, W), BF),
+            vmem((1, 16, 128, 128), BF),
+            vmem((1, 16, 64, 128), BF),
+            vmem((2, 16, 64, 640), BF),
             vmem((2, SEQ, D), BF),
             vmem((2, SEQ, D), BF),
             vmem((2, SEQ, W), F32),
@@ -579,15 +573,15 @@
             vmem((2, SEQ, 128), F32),
             vmem((2, 5, SEQ, W), F32),
             vmem((2, SEQ, 128), F32),
-            *exchange_buffers((HALF, W), 2),
-            *exchange_buffers((64, 2 * SEQ), 4),
-            dma((ROUNDS, 2, 8)),
-            dma((ROUNDS, 2, 8)),
-            dma((4, 8)),
-            dma((4, 8)),
-            dma((4, 10)),
-            dma((4, 10)),
-            dma((17,)),
+            *exchange_buffers((HALF, W), (4, 2)),
+            *exchange_buffers((64, 2 * SEQ), (16,)),
+            dma((ROUNDS,)),
+            dma((ROUNDS, 7)),
+            dma((4,)),
+            dma((4, 5)),
+            dma((4,)),
+            dma((4, 4)),
+            dma((16,)),
         ],
         compiler_params=pltpu.CompilerParams(
             collective_id=0, has_side_effects=True, vmem_limit_bytes=62 * 1024 * 1024

time: 105 us -> 99.3 us (0.946)
  Pallas kernels: 103 us -> 97.3 us
    pallas_call x1, Pallas kernels: 103 us -> 97.3 us  [on_device(): pl.pallas_call(kernel, out_shape=jax.ShapeDtypeStruct(tokens.shape, BF),...]
where the time goes in v5:
time: 99.3 us; the launch traced here: 99.1 us
  Pallas kernels  97.3 us (98%)
  local copies, waits for them, and re-layouts  1.77 us (2%)
    pallas_call x1, Pallas kernels, on_device(): pl.pallas_call(kernel, out_shape=jax.ShapeDtypeStruct(tokens.shape, BF),...  97.3 us

profile of v5, /device:TPU:1, one launch (start us, length us, event | category | flops | bytes accessed | tf_op | source)
XLA Modules:
  0.0 99.1 jit_solution(16238822305189952049)
XLA Ops:
  0.0 97.3 %layer.1 = bf16[2,384,256]{2,1,0:T(8,128)(2,1)} custom-call(bf16[2,384,256]{2,1,0:T(8,128)(2,1)} %tok_h.1, f32[16,128]{1,0:T(8,128)} %bitcast.8, f32[128,256]{1,0:T(8,128)} %wb_h.1, f32[128,256]{1,0:T(8,128)} %wc_h.1, f32[128,256]{1,0:T(8,128)} %wv_h.1, f32[3,256]{1,0:T(4,128)} %insc_h.1, f32[3,256]{1,0:T(4,128)} %mtaps_h.1, f32[256,128]{1,0:T(8,128)} %wm_h.1, ...), custom_call_target="tpu_custom_call" | custom-call | tf_op jit(solution)/shard_map/layer/pallas_call | solution.py:554
  97.3 1.8 %copy.18 = bf16[2,384,256]{2,1,0:T(8,128)(2,1)} copy(bf16[2,384,256]{2,1,0:T(8,128)(2,1)} %layer.1) | data formatting | bytes 786432

commit v6 on v5

--- a/solution.py
+++ b/solution.py
@@ -315,7 +315,7 @@
 
     def ffn_unit(h):
         return Unit(
-            h, 2 + h, sb2, rb2, lambda k, d: keep2[h, 4 * order[k] + 2 * core + d], fbuf2, nbuf2, rf2, rn2
+            h, 2 + h, sb2, rb2, lambda k, d: keep2[h, 2 * k + d], fbuf2, nbuf2, rf2, rn2
         )
 
     def dot(a, b):
@@ -378,18 +378,25 @@
         active[832:896, tokens_of(s)] = act
         active[704:832, tokens_of(s)] = jnp.zeros((128, SEQ), BF)
 
-    def down_parts(h, unit):
+    def down_parts(h, unit, cc):
         lo = 640 + 128 * h
         acts = jnp.concatenate([active[0:640, :], active[lo : lo + 128, :]], axis=0)
-        for first, ks in ((2, (0, 1)), (0, (2, 3))):
-            places = slice(4 * first, 4 * first + 8)
-            mat = jnp.concatenate(
-                [g_d[h, places].reshape(512, 640), g_dt[0, places].reshape(512, 128)], axis=1
-            )
-            keep2[h, places] = dot(mat, acts).reshape(8, 64, 2 * SEQ)
-            for k in ks:
-                piece = keep2[h, pl.ds(4 * order[k] + 2 * (1 - core), 2)].astype(BF)
-                sb2[8 * h + 2 * k : 8 * h + 2 * k + 2] = piece
+        mat = jnp.concatenate(
+            [
+                jnp.concatenate(
+                    [g_d[h, 4 * place + 2 * cc + j], g_dt[0, 4 * place + 2 * cc + j]], axis=1
+                )
+                for place in order
+                for j in range(2)
+            ],
+            axis=0,
+        )
+        term = dot(mat, acts).reshape(8, 64, 2 * SEQ)
+        if cc is core:
+            keep2[h] = term
+        else:
+            sb2[8 * h : 8 * h + 8] = term.astype(BF)
+            for k in range(4):
                 unit.part(k)
 
     own = cols_of(1, core)
@@ -479,18 +486,18 @@
     s4(9)
     up_first(0, (0, 1, 2, 3))
     gather_near(3, rfull, 1)
-    s2(12)
     s3(11)
     s4(10)
-    gather_far(2, rfull, 0)
     done(8)
     done(9)
     up_first(0, (4, 5))
+    s2(12)
+    gather_far(2, rfull, 0)
     near_done(3, rfull, 1)
     add_squares(rfull, 1, (0, 3))
     up_first(1, (0, 1, 2, 3, 4, 5))
-    s3(12)
     gather_far(3, rfull, 1)
+    s4(11)
 
     def finish(s):
         far_done(2 + s, rfull, s)
@@ -499,19 +506,22 @@
         up_second(s)
 
     finish(0)
-    s4(11)
+    s3(12)
     finish(1)
-    s4(12)
     done(10)
     done(11)
     v0, v1 = ffn_unit(0), ffn_unit(1)
-    down_parts(0, v0)
+    other = 1 - core
+    down_parts(0, v0, other)
+    s4(12)
+    down_parts(0, v0, core)
     v0.far()
     v0.near()
     done(12)
-    down_parts(1, v1)
+    down_parts(1, v1, other)
+    v0.last()
+    down_parts(1, v1, core)
     v1.far()
-    v0.last()
     v1.near()
     v1.last()
     for src, ssem in sent:
@@ -574,7 +584,7 @@
             vmem((2, 5, SEQ, W), F32),
             vmem((2, SEQ, 128), F32),
             *exchange_buffers((HALF, W), (4, 2)),
-            *exchange_buffers((64, 2 * SEQ), (16,)),
+            *exchange_buffers((64, 2 * SEQ), (8,)),
             dma((ROUNDS,)),
             dma((ROUNDS, 7)),
             dma((4,)),

time: 99.3 us -> 97.9 us (0.986); the launches traced: 99.1 us -> 96 us
  Pallas kernels: 97.3 us -> 94.3 us
    pallas_call x1, Pallas kernels: 97.3 us -> 94.3 us  [on_device(): pl.pallas_call(kernel, out_shape=jax.ShapeDtypeStruct(tokens.shape, BF),...]
where the time goes in v6:
time: 97.9 us; the launch traced here: 96 us
  Pallas kernels  94.3 us (96%)
  local copies, waits for them, and re-layouts  1.77 us (2%)
    pallas_call x1, Pallas kernels, on_device(): pl.pallas_call(kernel, out_shape=jax.ShapeDtypeStruct(tokens.shape, BF),...  94.3 us

profile of v6, /device:TPU:1, one launch (start us, length us, event | category | flops | bytes accessed | tf_op | source)
XLA Modules:
  0.0 96.0 jit_solution(13288881182007879833)
XLA Ops:
  0.0 94.3 %layer.1 = bf16[2,384,256]{2,1,0:T(8,128)(2,1)} custom-call(bf16[2,384,256]{2,1,0:T(8,128)(2,1)} %tok_h.1, f32[16,128]{1,0:T(8,128)} %bitcast.8, f32[128,256]{1,0:T(8,128)} %wb_h.1, f32[128,256]{1,0:T(8,128)} %wc_h.1, f32[128,256]{1,0:T(8,128)} %wv_h.1, f32[3,256]{1,0:T(4,128)} %insc_h.1, f32[3,256]{1,0:T(4,128)} %mtaps_h.1, f32[256,128]{1,0:T(8,128)} %wm_h.1, ...), custom_call_target="tpu_custom_call" | custom-call | tf_op jit(solution)/shard_map/layer/pallas_call | solution.py:564
  94.3 1.8 %copy.18 = bf16[2,384,256]{2,1,0:T(8,128)(2,1)} copy(bf16[2,384,256]{2,1,0:T(8,128)(2,1)} %layer.1) | data formatting | bytes 786432

commit v7 on v6

--- a/solution.py
+++ b/solution.py
@@ -449,18 +449,19 @@
     s3(6)
     mix_parts(1, u1)
     s4(5)
+    s1(9)
+    s1(10)
     u1.far()
+    s2(8)
     u0.last()
     u1.near()
-    s1(9)
-    s2(8)
     s3(7)
     s4(6)
-    s1(10)
+    s1(11)
+    s2(9)
     u1.last()
-    s2(9)
-    s1(11)
     s3(8)
+    s2(10)
 
     def residual(s, unit):
         unit.landed()
@@ -471,33 +472,33 @@
 
     residual(0, u0)
     s4(7)
-    s2(10)
+    s1(12)
     residual(1, u1)
-    s1(12)
     s3(9)
     s2(11)
+    s3(10)
     gather_near(2, rfull, 0)
     s4(8)
-    s3(10)
     near_done(2, rfull, 0)
     add_squares(rfull, 0, (0, 3))
     for r in range(4, 8):
         done(r)
     s4(9)
+    s2(12)
     up_first(0, (0, 1, 2, 3))
+    s3(11)
     gather_near(3, rfull, 1)
-    s3(11)
     s4(10)
     done(8)
     done(9)
     up_first(0, (4, 5))
-    s2(12)
     gather_far(2, rfull, 0)
+    s3(12)
     near_done(3, rfull, 1)
     add_squares(rfull, 1, (0, 3))
     up_first(1, (0, 1, 2, 3, 4, 5))
+    s4(11)
     gather_far(3, rfull, 1)
-    s4(11)
 
     def finish(s):
         far_done(2 + s, rfull, s)
@@ -506,22 +507,21 @@
         up_second(s)
 
     finish(0)
-    s3(12)
     finish(1)
+    s4(12)
     done(10)
     done(11)
     v0, v1 = ffn_unit(0), ffn_unit(1)
     other = 1 - core
     down_parts(0, v0, other)
-    s4(12)
     down_parts(0, v0, core)
     v0.far()
     v0.near()
     done(12)
     down_parts(1, v1, other)
-    v0.last()
     down_parts(1, v1, core)
     v1.far()
+    v0.last()
     v1.near()
     v1.last()
     for src, ssem in sent:
@@ -563,7 +563,7 @@
     dma = pltpu.SemaphoreType.DMA
     return pl.pallas_call(
         kernel,
-        out_shape=jax.ShapeDtypeStruct(tokens.shape, BF),
+        out_shape=vmem(tokens.shape, BF),
         in_specs=[pl.BlockSpec(memory_space=pl.ANY)] * len(args),
         out_specs=pl.BlockSpec(memory_space=pltpu.VMEM),
         scratch_shapes=[
@@ -594,7 +594,7 @@
             dma((16,)),
         ],
         compiler_params=pltpu.CompilerParams(
-            collective_id=0, has_side_effects=True, vmem_limit_bytes=62 * 1024 * 1024
+            collective_id=0, has_side_effects=True, vmem_limit_bytes=60 * 1024 * 1024
         ),
         name="layer",
     )(*args)

time: 97.9 us -> 95.6 us (0.977); the launches traced: 96 us -> 95.5 us
  local copies, waits for them, and re-layouts: 1.77 us -> 0.75 us
    unnamed x1, local copies, waits for them, and re-layouts: 1.77 us -> 0.75 us
where the time goes in v7:
time: 95.6 us; the launch traced here: 95.5 us
  Pallas kernels  94.7 us (99%)
    pallas_call x1, Pallas kernels, on_device(): pl.pallas_call(kernel, out_shape=vmem(tokens.shape, BF), in_specs=[pl.Blo...  94.7 us

profile of v7, /device:TPU:1, one launch (start us, length us, event | category | flops | bytes accessed | tf_op | source)
XLA Modules:
  0.0 95.5 jit_solution(7519080708159958618)
XLA Ops:
  0.0 94.7 %layer.1 = bf16[2,384,256]{2,1,0:T(8,128)(2,1)S(1)} custom-call(bf16[2,384,256]{2,1,0:T(8,128)(2,1)} %tok_h.1, f32[16,128]{1,0:T(8,128)} %bitcast.8, f32[128,256]{1,0:T(8,128)} %wb_h.1, f32[128,256]{1,0:T(8,128)} %wc_h.1, f32[128,256]{1,0:T(8,128)} %wv_h.1, f32[3,256]{1,0:T(4,128)} %insc_h.1, f32[3,256]{1,0:T(4,128)} %mtaps_h.1, f32[256,128]{1,0:T(8,128)} %wm_h.1, ...), custom_call_target="tpu_custom_call" | custom-call | tf_op jit(solution)/shard_map/layer/pallas_call | solution.py:564
  94.7 0.7 copy.18

commit v8 on v7

--- a/solution.py
+++ b/solution.py
@@ -150,7 +150,7 @@
         return lo, half, lo, lo + half // 2, half // 2, pos[h], pos[1 - h]
 
     def hop(r, h, stage, piece, axis, d):
-        push(piece, piece, y_send.at[r], y_recv.at[r, 2 * stage + h if stage < 3 else 6], dev_axis[axis][d])
+        push(piece, piece, y_send.at[r], y_recv.at[r, stage], dev_axis[axis][d])
 
     def across(r, h, p_at):
         lo, half, up, dn, quarter, p, q = geometry(r, h)
@@ -170,35 +170,36 @@
     def s2(r):
         if not 0 <= r < ROUNDS:
             return
+        arrived(some(r, 4, rounds[r][2] // 2), y_recv.at[r, 0])
         for h in range(2):
             lo, half, up, dn, quarter, p, q = geometry(r, h)
-            arrived(some(r, 2, half), y_recv.at[r, h])
             for d, at, part in ((0, (p + 3) % 4, up), (1, (p + 1) % 4, dn)):
                 hop(r, h, 1, block(r, h, at, q, part, quarter), h, d)
+        for h in range(2):
+            lo, half, up, dn, quarter, p, q = geometry(r, h)
             for at in ((p + 3) % 4, (p + 1) % 4):
                 across(r, h, at)
 
     def s3(r):
         if not 0 <= r < ROUNDS:
             return
+        arrived(some(r, 4, rounds[r][2] // 4), y_recv.at[r, 1])
         for h in range(2):
-            lo, half, up, dn, quarter, p, q = geometry(r, h)
-            arrived(some(r, 2, quarter), y_recv.at[r, 2 + h])
-            across(r, h, (p + 2) % 4)
+            across(r, h, (pos[h] + 2) % 4)
 
     def s4(r):
         if not 0 <= r < ROUNDS:
             return
+        arrived(some(r, 16, rounds[r][2] // 2), y_recv.at[r, 2])
         for h in range(2):
             lo, half, up, dn, quarter, p, q = geometry(r, h)
-            arrived(some(r, 8, half), y_recv.at[r, 4 + h])
             for d, at, part in ((0, (q + 3) % 4, up), (1, (q + 1) % 4, dn)):
                 for k in range(4):
                     hop(r, h, 3, block(r, h, k, at, part, quarter), 1 - h, d)
         sent.append((some(r, 15, rounds[r][2]), y_send.at[r]))
 
     def done(r):
-        arrived(some(r, 16, rounds[r][2] // 4), y_recv.at[r, 6])
+        arrived(some(r, 16, rounds[r][2] // 4), y_recv.at[r, 3])
 
     def ahead(k):
         s1(k + 2)
@@ -586,7 +587,7 @@
             *exchange_buffers((HALF, W), (4, 2)),
             *exchange_buffers((64, 2 * SEQ), (8,)),
             dma((ROUNDS,)),
-            dma((ROUNDS, 7)),
+            dma((ROUNDS, 4)),
             dma((4,)),
             dma((4, 5)),
             dma((4,)),

time: 95.6 us -> 94 us (0.983)
  Pallas kernels: 94.7 us -> 93.1 us
    pallas_call x1, Pallas kernels: 94.7 us -> 93.1 us  [on_device(): pl.pallas_call(kernel, out_shape=vmem(tokens.shape, BF), in_specs=[pl.Blo...]
where the time goes in v8:
time: 94 us; the launch traced here: 93.9 us
  Pallas kernels  93.1 us (99%)
    pallas_call x1, Pallas kernels, on_device(): pl.pallas_call(kernel, out_shape=vmem(tokens.shape, BF), in_specs=[pl.Blo...  93.1 us

profile of v8, /device:TPU:1, one launch (start us, length us, event | category | flops | bytes accessed | tf_op | source)
XLA Modules:
  0.0 93.9 jit_solution(14981134310635173122)
XLA Ops:
  0.0 93.1 %layer.1 = bf16[2,384,256]{2,1,0:T(8,128)(2,1)S(1)} custom-call(bf16[2,384,256]{2,1,0:T(8,128)(2,1)} %tok_h.1, f32[16,128]{1,0:T(8,128)} %bitcast.8, f32[128,256]{1,0:T(8,128)} %wb_h.1, f32[128,256]{1,0:T(8,128)} %wc_h.1, f32[128,256]{1,0:T(8,128)} %wv_h.1, f32[3,256]{1,0:T(4,128)} %insc_h.1, f32[3,256]{1,0:T(4,128)} %mtaps_h.1, f32[256,128]{1,0:T(8,128)} %wm_h.1, ...), custom_call_target="tpu_custom_call" | custom-call | tf_op jit(solution)/shard_map/layer/pallas_call | solution.py:565
  93.1 0.7 copy.18
